TPU v7x, 128 devices: a whole 4x4x4 slice. The times are simulated.
128 devices in a mesh: ep: 128 (over z, y, x, core).
Axes of the slice: x: 4, y: 4, z: 4, core: 2. Of those that a mesh axis runs over, the one named last changes fastest.
Arguments:
- hidden: bfloat16 [1024, 2048], P('ep'), may hold values from -6 to 6
- lengths: int32 [1024], P('ep'), may hold values from 1 to 1024
- key_cache: bfloat16 [1024, 1024, 128], P('ep'), may hold values from -6 to 6
- value_cache: bfloat16 [1024, 1024, 128], P('ep'), may hold values from -6 to 6
- norm_gain: bfloat16 [2048], replicated, may hold values from 0.099609375 to 1.8984375
- w_query: bfloat16 [2048, 1024], replicated, may hold values from -0.125 to 0.125
- w_key: bfloat16 [2048, 128], replicated, may hold values from -0.125 to 0.125
- w_value: bfloat16 [2048, 128], replicated, may hold values from -0.125 to 0.125
- head_bias: float32 [16], replicated, may hold values from -7 to -2
- w_out: bfloat16 [1024, 2048], replicated, may hold values from -0.1875 to 0.1875
- ffn_gain: bfloat16 [2048], replicated, may hold values from 0.099609375 to 1.8984375
- routing: int32 [1024, 2], P('ep'), may hold values from 0 to 7, all different within a row; in each aligned block of 8 rows (0 to 7, 8 to 15, ...) at most 4 rows name the same one
- route_w: bfloat16 [1024, 2], P('ep'), may hold values from 0.19921875 to 1
- w_gate: bfloat16 [128, 2048, 352], P('ep'), may hold values from -0.125 to 0.125
- w_up: bfloat16 [128, 2048, 352], P('ep'), may hold values from -0.125 to 0.125
- w_down: bfloat16 [128, 352, 2048], P('ep'), may hold values from -0.078125 to 0.078125
Outputs:
- mixed: bfloat16 [1024, 2048], P('ep')
- new_key: bfloat16 [1024, 128], P('ep')
- new_value: bfloat16 [1024, 128], P('ep')
Inputs may be any that keep to these rules, and one draw needn't show every extreme that they name: `lengths`: positions at and beyond a sequence's length are unused. `routing`: the 2 experts of a token differ; among the rows of one device at most 4 tokens name the same expert.
All inputs are finite; a program needn't handle non-finite values.
Results may differ from a plain program's by a relative error of at most 0.013.
Values may be sent and summed in bfloat16 or wider, within the bound.
A program may use at most 128 MiB of HBM per device.

v0:
```python
import jax
import jax.numpy as jnp
from jax import lax
from jax.sharding import PartitionSpec as P

D = 2048
HEADS = 16
HD = 64
KVH = 2
EXPERTS = 8
CAP = 4


def rms_norm(value, gain):
    wide = value.astype(jnp.float32)
    scaled = wide * lax.rsqrt(jnp.mean(wide * wide, axis=-1, keepdims=True) + 1e-06)
    return (scaled * gain.astype(jnp.float32)).astype(jnp.bfloat16)


def expert_rows(rows, gate_w, up_w):
    gate = jnp.dot(rows, gate_w, preferred_element_type=jnp.float32)
    upper = jnp.dot(rows, up_w, preferred_element_type=jnp.float32)
    return (jax.nn.silu(gate) * upper).astype(jnp.bfloat16)


def later_sums(keep_terms, cache):
    span_len = 128
    nblocks = cache // span_len
    lead = keep_terms.shape[:-1]
    blocked = keep_terms.reshape(lead + (nblocks, span_len))
    position = jnp.arange(span_len, dtype=jnp.int32)
    triangle = (position[:, None] > position[None, :]).astype(jnp.float32)
    within = jnp.einsum("...bj,ji->...bi", blocked, triangle)
    totals = jnp.sum(blocked, axis=-1)
    block_ids = jnp.arange(nblocks, dtype=jnp.int32)
    block_tri = (block_ids[:, None] > block_ids[None, :]).astype(jnp.float32)
    beyond = jnp.einsum("...j,ji->...i", totals, block_tri)
    return (within + beyond[..., None]).reshape(lead + (cache,))


def local(
    hidden,
    lengths,
    key_cache,
    value_cache,
    norm_gain,
    w_query,
    w_key,
    w_value,
    head_bias,
    w_out,
    ffn_gain,
    routing,
    route_w,
    w_gate,
    w_up,
    w_down,
):
    count = hidden.shape[0]
    cache = key_cache.shape[1]
    groups = HEADS // KVH
    normed = rms_norm(hidden, norm_gain)
    query = jnp.dot(normed, w_query, preferred_element_type=jnp.float32).astype(jnp.bfloat16)
    new_key = jnp.dot(normed, w_key, preferred_element_type=jnp.float32).astype(jnp.bfloat16)
    new_value = jnp.dot(normed, w_value, preferred_element_type=jnp.float32).astype(jnp.bfloat16)
    q_heads = query.reshape(count, KVH, groups, HD)
    k_heads = key_cache.reshape(count, cache, KVH, HD)
    v_heads = value_cache.reshape(count, cache, KVH, HD)
    scores = jnp.einsum(
        "sgrd,scgd->sgrc", q_heads, k_heads, preferred_element_type=jnp.float32
    ) * HD ** (-0.5)
    scores = scores + head_bias.reshape(KVH, groups)[None, :, :, None]
    mask = (jnp.arange(cache, dtype=jnp.int32)[None, :] < lengths[:, None])[:, None, None, :]
    keep = jnp.where(mask, jax.nn.log_sigmoid(-scores), 0.0)
    after = later_sums(keep, cache)
    weight = jnp.where(mask, jnp.exp(jax.nn.log_sigmoid(scores) + after), 0.0).astype(jnp.bfloat16)
    attended = jnp.einsum("sgrc,scgd->sgrd", weight, v_heads, preferred_element_type=jnp.float32)
    attended = attended.reshape(count, HEADS * HD).astype(jnp.bfloat16)
    after_attention = (
        hidden.astype(jnp.float32) + jnp.dot(attended, w_out, preferred_element_type=jnp.float32)
    ).astype(jnp.bfloat16)
    expert_in = rms_norm(after_attention, ffn_gain)
    picked = (routing[:, :, None] == jnp.arange(EXPERTS, dtype=jnp.int32)[None, None, :]).astype(
        jnp.float32
    )
    table = jnp.sum(picked * route_w.astype(jnp.float32)[:, :, None], axis=1)
    slices = lax.axis_size("ep") // EXPERTS
    named = jnp.sum(picked, axis=1)
    lower = (jnp.arange(count)[None, :] <= jnp.arange(count)[:, None]).astype(jnp.float32)
    rank = jnp.dot(lower, named) - 1.0
    slot_ids = jnp.arange(CAP, dtype=jnp.float32)
    place = named.T[:, None, :] * (rank.T[:, None, :] == slot_ids[None, :, None]).astype(
        jnp.float32
    )
    packed = jnp.einsum(
        "ect,td->ecd", place.astype(jnp.bfloat16), expert_in, preferred_element_type=jnp.float32
    ).astype(jnp.bfloat16)
    outgoing = jnp.broadcast_to(packed[:, None], (EXPERTS, slices, CAP, D)).reshape(
        EXPERTS * slices, CAP, D
    )
    received = lax.all_to_all(outgoing, "ep", split_axis=0, concat_axis=0, tiled=True)
    sources, items, width = received.shape
    act = expert_rows(received.reshape(sources * items, width), w_gate[0], w_up[0])
    out = jnp.dot(act, w_down[0], preferred_element_type=jnp.float32)
    partial_value = out.reshape(sources, items, width)
    returned = lax.all_to_all(
        partial_value.astype(jnp.bfloat16), "ep", split_axis=0, concat_axis=0, tiled=True
    ).astype(partial_value.dtype)
    per_expert = jnp.sum(returned.reshape(EXPERTS, slices, CAP, D), axis=1)
    scale = place * table.T[:, None, :]
    combined = jnp.einsum("ect,ecd->td", scale, per_expert, preferred_element_type=jnp.float32)
    mixed = (after_attention.astype(jnp.float32) + combined).astype(jnp.bfloat16)
    return (mixed, new_key, new_value)


def solution(mesh):
    in_specs = (
        P("ep", None),
        P("ep"),
        P("ep", None, None),
        P("ep", None, None),
        P(),
        P(),
        P(),
        P(),
        P(),
        P(),
        P(),
        P("ep", None),
        P("ep", None),
        P("ep", None, None),
        P("ep", None, None),
        P("ep", None, None),
    )
    out_specs = (P("ep", None), P("ep", None), P("ep", None))
    return jax.shard_map(local, mesh=mesh, in_specs=in_specs, out_specs=out_specs, check_vma=False)
```

profile of v0, /device:TPU:1, one launch (start us, length us, event | category | flops | bytes accessed | tf_op | source)
XLA Modules:
  0.0 119.8 jit_solution(9731533430188144241)
XLA Ops:
  0.6 0.0 copy-start
  0.6 1.0 fusion.30
  1.7 1.3 %add.58 = f32[2,8]{1,0:T(2,128)} reshape(f32[16]{0:T(128)} %param.24) | data formatting | bytes 128 | tf_op jit(solution)/shard_map/add | solution.py:72
  3.0 0.7 convert_element_type.77
  3.6 1.3 %select_reduce_fusion = (f32[8,8]{1,0:T(8,128)}, f32[8,8]{1,0:T(8,128)S(1)}) fusion(f32[8,2]{0,1:T(2,128)S(1)} %convert_element_type.77, s32[8,2]{0,1:T(2,128)} %param.27), kind=kLoop, calls=%fused_computation.56 | loop fusion | flops 512 | bytes 640 | tf_op jit(solution)/shard_map/reduce_sum | solution.py:86
  5.0 0.6 copy-done.5
  5.6 0.2 convolution_add_fusion.2
  5.7 0.7 copy.67
  6.4 0.7 convert_element_type.68
  7.1 0.7 iota_compare_fusion.1
  7.8 1.3 %convert_element_type.79 = f32[2048]{0:T(1024)} convert(bf16[2048]{0:T(1024)(128)(2,1)} %param.26) | non-fusion elementwise | flops 2048 | bytes 12288 | tf_op jit(solution)/shard_map/convert_element_type | solution.py:17
  9.1 2.9 %convolution_convert_fusion.3 = bf16[8,1024]{1,0:T(8,128)(2,1)S(1)} fusion(bf16[2048,1024]{1,0:T(8,128)(2,1)} %param.21, bf16[8,2048]{1,0:T(8,128)(2,1)} %param.16, f32[2048]{0:T(1024)S(1)} %convert_element_type.68, f32[8]{0:T(128)S(1)} %add_rsqrt_fusion.1), kind=kOutput, calls=%fused_computation.22 | convolution fusion | flops 33628160 | bytes 4251680 | tf_op jit(solution)/shard_map/dot_general | solution.py:63
  12.0 0.7 reshape.80
  12.7 2.9 %copy.63 = bf16[8,1024,128]{1,2,0:T(8,128)(2,1)S(1)} copy(bf16[8,1024,128]{2,1,0:T(8,128)(2,1)} %param.18) | data formatting | bytes 4194304 | tf_op args[2]
  15.6 1.1 fusion.15
  16.7 0.0 copy-start.1
  16.7 0.8 copy-done.1
  17.5 0.5 fusion.55
  18.0 0.2 fusion.47
  18.2 0.2 convolution_add_fusion.1
  18.4 0.9 reshape.83
  19.3 2.9 %copy.66 = bf16[8,1024,128]{1,2,0:T(8,128)(2,1)S(1)} copy(bf16[8,1024,128]{2,1,0:T(8,128)(2,1)} %param.19) | data formatting | bytes 4194304 | tf_op args[3]
  22.2 2.5 %convolution_convert_fusion.2 = bf16[8,2,8,64]{3,2,1,0:T(8,128)(2,1)} fusion(bf16[8,1024,2,64]{1,3,2,0:T(8,128)(2,1)S(1)} %bitcast.60, f32[8,2,8,1024]{3,2,1,0:T(8,128)} %reshape.83, f32[8,2,8,1024]{3,2,1,0:T(8,128)} %copy-done.1, pred[8,1024]{1,0:T(8,128)(4,1)S(1)} %iota_compare_fusion.1), kind=kOutput, calls=%fused_computation.21 | convolution fusion | flops 18227200 | bytes 3170304 | tf_op jit(solution)/shard_map/sgrc,scgd->sgrd/dot_general | solution.py:77
  24.6 0.9 convert_element_type.73
  25.5 0.0 copy-start.7
  25.5 0.0 copy-start.8
  25.5 3.0 %multiply_reduce_fusion = (f32[8]{0:T(128)S(1)}, f32[8,2048]{1,0:T(8,128)S(1)}) fusion(bf16[8,1024]{1,0:T(8,128)(2,1)S(1)} %convert_element_type.73, bf16[1024,2048]{1,0:T(8,128)(2,1)} %param.25, bf16[8,2048]{1,0:T(8,128)(2,1)} %param.16), kind=kOutput, calls=%fused_computation.45 | convolution fusion | flops 33652728 | bytes 4309024 | tf_op jit(solution)/shard_map/dot_general | solution.py:80
  28.5 0.2 convolution_convert_fusion.1
  28.8 0.3 copy-done.3
  29.1 0.1 copy.69
  29.2 1.0 broadcast_in_dim.17
  30.3 41.8 %all_to_all.10 = bf16[128,4,2048]{2,1,0:T(4,128)(2,1)S(1)} all-to-all(bf16[128,4,2048]{2,1,0:T(4,128)(2,1)S(1)} %bitcast.62), channel_id=1, replica_groups=mesh['ep'=128] {'ep'}, dimensions={0} | all-to-all | bytes 4194304 | tf_op jit(solution)/shard_map/all_to_all | solution.py:101
  72.0 2.1 %reshape.86 = bf16[512,2048]{1,0:T(8,128)(2,1)} reshape(bf16[128,4,2048]{2,1,0:T(4,128)(2,1)S(1)} %all_to_all.10) | data formatting | bytes 4194304 | tf_op jit(solution)/shard_map/reshape | solution.py:103
  74.1 3.1 %fusion.7 = f32[512,352]{0,1:T(8,128)S(1)} fusion(bf16[512,2048]{1,0:T(8,128)(2,1)} %reshape.86, bf16[1,2048,352]{1,2,0:T(8,128)(2,1)} %param.29), kind=kOutput, calls=%fused_computation.14 | convolution fusion | flops 738197504 | bytes 4259840 | tf_op jit(solution)/shard_map/dot_general | solution.py:21
  77.2 0.0 copy-done.2
  77.2 0.0 copy-done.11
  77.2 1.0 fusion.12
  78.2 0.2 copy.70
  78.4 0.1 dot_general.54
  78.5 1.3 %convolution_convert_fusion = bf16[128,4,2048]{2,0,1:T(8,128)(2,1)S(1)} fusion(bf16[1,352,2048]{2,1,0:T(8,128)(2,1)S(1)} %copy-done, bf16[128,4,352]{2,1,0:T(4,128)(2,1)S(1)} %dot_general.54), kind=kOutput, calls=%fused_computation.1 | convolution fusion | flops 739246080 | bytes 3899392 | tf_op jit(solution)/shard_map/dot_general | solution.py:104
  79.8 3.0 %copy.72 = bf16[128,4,2048]{2,1,0:T(4,128)(2,1)} copy(bf16[128,4,2048]{2,0,1:T(8,128)(2,1)S(1)} %convolution_convert_fusion) | data formatting | bytes 4194304 | tf_op jit(solution)/shard_map/convert_element_type | solution.py:107
  82.8 4.4 %all-to-all-start.1 = ((bf16[128,4,2048]{2,1,0:T(4,128)(2,1)}), bf16[128,4,2048]{2,1,0:T(4,128)(2,1)S(1)}, u32[]{:S(2)}, u32[]{:S(2)}) async-start(bf16[128,4,2048]{2,1,0:T(4,128)(2,1)} %copy.72), calls=%async_computation.1 | async-start | bytes 4194304 | tf_op jit(solution)/shard_map/all_to_all | solution.py:106
  87.2 1.9 %convolution_convert_fusion.5 = bf16[8,128]{1,0:T(8,128)(2,1)} fusion(bf16[2048,128]{1,0:T(8,128)(2,1)} %param.22, bf16[8,2048]{1,0:T(8,128)(2,1)} %param.16, f32[2048]{0:T(1024)S(1)} %convert_element_type.68, f32[8]{0:T(128)} %copy-done.10), kind=kOutput, calls=%fused_computation.25 | convolution fusion | flops 4260864 | bytes 567328 | tf_op jit(solution)/shard_map/dot_general | solution.py:64
  89.1 1.9 %convolution_convert_fusion.4 = bf16[8,128]{1,0:T(8,128)(2,1)} fusion(bf16[2048,128]{1,0:T(8,128)(2,1)} %param.23, bf16[8,2048]{1,0:T(8,128)(2,1)} %param.16, f32[2048]{0:T(1024)S(1)} %convert_element_type.68, f32[8]{0:T(128)} %copy-done.10), kind=kOutput, calls=%fused_computation.24 | convolution fusion | flops 4260864 | bytes 567328 | tf_op jit(solution)/shard_map/dot_general | solution.py:65
  91.0 26.8 %all-to-all-done.1 = bf16[128,4,2048]{2,1,0:T(4,128)(2,1)S(1)} async-done(((bf16[128,4,2048]{2,1,0:T(4,128)(2,1)}), bf16[128,4,2048]{2,1,0:T(4,128)(2,1)S(1)}, u32[]{:S(2)}, u32[]{:S(2)}) %all-to-all-start.1) | async-done | bytes 2097184 | tf_op jit(solution)/shard_map/all_to_all | solution.py:106
  117.8 1.1 convert_reduce_fusion
  118.9 0.0 copy-done.9
  118.9 0.9 fusion.1
  (16 shorter events, 0.0 us)
Async XLA Ops:
  0.6 77.9 %copy-start = (bf16[1,352,2048]{2,1,0:T(8,128)(2,1)S(1)}, bf16[1,352,2048]{2,1,0:T(8,128)(2,1)}, u32[]{:S(2)}) copy-start(bf16[1,352,2048]{2,1,0:T(8,128)(2,1)} %param.31) | copy-start | bytes 4325380
  1.7 10.3 %copy-start.10 = (f32[8]{0:T(128)}, f32[8]{0:T(128)S(1)}, u32[]{:S(2)}) copy-start(f32[8]{0:T(128)S(1)} %add_rsqrt_fusion.1) | copy-start | bytes 100
  5.0 0.6 copy-start.5
  16.7 0.8 copy-start.1
  25.5 3.0 %copy-start.6 = (f32[8,8]{1,0:T(8,128)S(1)}, f32[8,8]{1,0:T(8,128)}, u32[]{:S(2)}) copy-start(f32[8,8]{1,0:T(8,128)} %copy-done.5) | copy-start | bytes 772
  25.5 3.0 %copy-start.7 = (f32[8,8]{0,1:T(8,128)S(1)}, f32[8,8]{0,1:T(8,128)}, u32[]{:S(2)}) copy-start(f32[8,8]{0,1:T(8,128)} %copy.67) | copy-start | bytes 772
  25.5 3.0 %copy-start.8 = (f32[2048]{0:T(1024)S(1)}, f32[2048]{0:T(1024)}, u32[]{:S(2)}) copy-start(f32[2048]{0:T(1024)} %convert_element_type.79) | copy-start | bytes 24580
  28.5 0.6 copy-start.3
  74.1 3.1 %copy-start.2 = (bf16[512,2048]{1,0:T(8,128)(2,1)S(1)}, bf16[512,2048]{1,0:T(8,128)(2,1)}, u32[]{:S(2)}) copy-start(bf16[512,2048]{1,0:T(8,128)(2,1)} %reshape.86) | copy-start | bytes 6291460
  74.1 3.1 %copy-start.11 = (bf16[1,2048,352]{1,2,0:T(8,128)(2,1)S(1)}, bf16[1,2048,352]{1,2,0:T(8,128)(2,1)}, u32[]{:S(2)}) copy-start(bf16[1,2048,352]{1,2,0:T(8,128)(2,1)} %param.30) | copy-start | bytes 4325380
  82.8 35.0 %all-to-all-start.1 = ((bf16[128,4,2048]{2,1,0:T(4,128)(2,1)}), bf16[128,4,2048]{2,1,0:T(4,128)(2,1)S(1)}, u32[]{:S(2)}, u32[]{:S(2)}) async-start(bf16[128,4,2048]{2,1,0:T(4,128)(2,1)} %copy.72), calls=%async_computation.1 | async-start | bytes 4194304 | tf_op jit(solution)/shard_map/all_to_all | solution.py:106
  91.0 27.9 %copy-start.9 = (f32[8,8]{1,0:T(8,128)S(1)}, f32[8,8]{1,0:T(8,128)}, u32[]{:S(2)}) copy-start(f32[8,8]{1,0:T(8,128)} %get-tuple-element.3) | copy-start | bytes 772
  117.8 1.1 copy-start.4
where the time goes:
time: 120 us
  blocking collectives  41.8 us (35%)
  waiting for transfers between devices  26.8 us (22%)
  matrix products  20.3 us (17%)
  local copies, waits for them, and re-layouts  18.4 us (15%)
  other arithmetic  7.23 us (6%)
  starting transfers between devices  4.41 us (4%)
    all_to_all x1, blocking collectives, local(): lax.all_to_all(outgoing, 'ep', split_axis=0, concat_axis=0, tiled=True)  41.8 us
    all_to_all x1, waiting for transfers between devices, local(): lax.all_to_all(partial_value.astype(jnp.bfloat16), 'ep', split_axis=0, co...  26.8 us
    unnamed x26, local copies, waits for them, and re-layouts  7.48 us
    all_to_all x1, starting transfers between devices, local(): lax.all_to_all(partial_value.astype(jnp.bfloat16), 'ep', split_axis=0, co...  4.41 us
    dot_general x1, matrix products, expert_rows(): gate = jnp.dot(rows, gate_w, preferred_element_type=jnp.float32)  3.08 us
    convert_element_type x1, local copies, waits for them, and re-layouts, local(): partial_value.astype(jnp.bfloat16)  2.97 us
    dot_general x1, matrix products, local(): jnp.dot(attended, w_out, preferred_element_type=jnp.float32)  2.96 us
    dot_general x1, matrix products, local(): jnp.dot(normed, w_query, preferred_element_type=jnp.float32)  2.89 us
  transfers between devices with their start and end apart: 1, of which 1 were waited for; matrix products, arithmetic and copies ran while one was open for 3% of the time, Pallas kernels for 0%

commit v1 on v0

v1 whole, which is shorter than its diff:
```python
import jax
import jax.numpy as jnp
from jax import lax
from jax.experimental import pallas as pl
from jax.experimental.pallas import tpu as pltpu
from jax.sharding import PartitionSpec as P

D = 2048
HEADS = 16
HD = 64
CACHE = 1024
SEQ = 8
FFD = 352
HALF = D // 2
F32 = jnp.float32
BF16 = jnp.bfloat16
MESH = pl.DeviceIdType.MESH
XOFF = (0, 3, 1, 2)
GROUPS = (0, 1, 3, 2)
QCHUNK = 4
OCHUNK = 2


def rms_norm(wide, gain):
    scaled = wide * lax.rsqrt(jnp.mean(wide * wide, axis=-1, keepdims=True) + 1e-06)
    return (scaled * gain).astype(BF16)


def kernel(
    hidden_ref, lengths_ref, key_hbm, value_hbm, norm_gain_ref, wq_hbm, wk_hbm, wv_hbm, bias_ref,
    wo_hbm, ffn_gain_ref, routing_ref, route_w_ref, wg_hbm, wu_hbm, wd_hbm,
    mixed_ref, newk_ref, newv_ref,
    wq, wk, wv, kc, vc, wo, wg, wu, wd,
    qs, zs, kp, osc, table, xin, xsend, msg, blk, pblk, ofull, obuf, pout, rbuf, ybuf, fsend, fbuf,
    lsem, tsend, trecv, xs_sem, xr_sem, d1s, d1r, ringp_s, ringp_r, ringm_s, ringm_r, rel_s, rel_r,
    ps, pr, os_, orr, ys, yr, fs, fr,
):
    me = lax.axis_index("ep")
    c = me % 2
    x = (me // 2) % 4
    y = (me // 8) % 4
    z = me // 32

    def dev(dz, dy, dx, core):
        return ((((z + dz) % 4) * 4 + (y + dy) % 4) * 4 + (x + dx) % 4) * 2 + core

    def remote(src, dst, ssem, rsem, target):
        return pltpu.make_async_remote_copy(
            src_ref=src, dst_ref=dst, send_sem=ssem, recv_sem=rsem,
            device_id=(target,), device_id_type=MESH,
        )

    def drain(ref, sem):
        pltpu.make_async_copy(ref, ref, sem).wait()

    loads = {}

    def load(name, src, dst):
        copy = pltpu.make_async_copy(src, dst, lsem.at[len(loads)])
        copy.start()
        loads[name] = copy

    qrows = D // QCHUNK
    for i in range(QCHUNK):
        load(("wq", i), wq_hbm.at[pl.ds(i * qrows, qrows)], wq.at[pl.ds(i * qrows, qrows)])
    load("key", key_hbm, kc)
    load("value", value_hbm, vc)
    orows = HEADS * HD // OCHUNK
    for i in range(OCHUNK):
        load(("wo", i), wo_hbm.at[pl.ds(i * orows, orows)], wo.at[pl.ds(i * orows, orows)])
    load("wk", wk_hbm, wk)
    load("wv", wv_hbm, wv)
    for i in range(2):
        half = (c + i) % 2
        load(("wg", i), wg_hbm.at[0, pl.ds(half * HALF, HALF)], wg.at[i])
        load(("wu", i), wu_hbm.at[0, pl.ds(half * HALF, HALF)], wu.at[i])
    for i in range(2):
        half = (c + i) % 2
        load(("wd", i), wd_hbm.at[0, :, pl.ds(pl.multiple_of(half * HALF, HALF), HALF)], wd.at[i])

    barrier = pltpu.get_barrier_semaphore()
    partners = [dev(d // 4, d % 4, 0, c) for d in range(1, 16)]
    row = [(k, core) for k in range(4) for core in range(2)]
    rowdev = [(k, o) for k in range(4) for o in range(2) if k + o > 0]
    partners += [dev(0, 0, 4 - XOFF[k], (c + o) % 2) for k, o in rowdev]
    for target in partners:
        pl.semaphore_signal(barrier, inc=1, device_id=(target,), device_id_type=MESH)

    lane = lax.broadcasted_iota(jnp.int32, (SEQ, 128), 1)
    plane = lane // 8
    lz = (z + plane // 4) % 4
    ly = (y + plane % 4) % 4
    lexpert = 2 * lz + ly // 2
    first, second = routing_ref[:, 0:1], routing_ref[:, 1:2]
    route_w = route_w_ref[...].astype(F32)
    is_first, is_second = lexpert == first, lexpert == second
    named = jnp.where(is_first | is_second, 1.0, 0.0).astype(F32)
    tri = (
        lax.broadcasted_iota(jnp.int32, (SEQ, SEQ), 0) >= lax.broadcasted_iota(jnp.int32, (SEQ, SEQ), 1)
    ).astype(F32)
    rank = jnp.dot(tri, named, preferred_element_type=F32)
    here = (jnp.abs(rank - 1.0 - (lane % 4).astype(F32)) < 0.5) & ((lane // 4) % 2 == c)
    weight = jnp.where(is_first, route_w[:, 0:1], jnp.where(is_second, route_w[:, 1:2], 0.0))
    table[0, c] = jnp.where(here, weight, 0.0)

    hidden = hidden_ref[...].astype(F32)
    normed = rms_norm(hidden, norm_gain_ref[...].astype(F32).reshape(1, D))
    query = jnp.zeros((SEQ, HEADS * HD), F32)
    for i in range(QCHUNK):
        loads[("wq", i)].wait()
        query = query + jnp.dot(
            normed[:, i * qrows : (i + 1) * qrows], wq[i * qrows : (i + 1) * qrows, :],
            preferred_element_type=F32,
        )
    query = query.astype(BF16).astype(F32)
    low = lax.broadcasted_iota(jnp.int32, (SEQ, 128), 1) < HD
    for j in range(8):
        tile = query[:, j * 128 : (j + 1) * 128]
        swapped = pltpu.roll(tile, HD, 1)
        if j < 4:
            even, odd = jnp.where(low, tile, 0.0), jnp.where(low, swapped, 0.0)
        else:
            even, odd = jnp.where(low, 0.0, swapped), jnp.where(low, 0.0, tile)
        qs[pl.ds(16 * j, 8), :] = even
        qs[pl.ds(16 * j + 8, 8), :] = odd

    pl.semaphore_wait(barrier, len(partners))
    tcopies = []
    for i, (k, o) in enumerate(rowdev):
        copy = remote(
            table.at[0, c], table.at[k, c], tsend.at[i], trecv.at[i],
            dev(0, 0, 4 - XOFF[k], (c + o) % 2),
        )
        copy.start()
        tcopies.append(copy)

    loads["key"].wait()
    sub = lax.broadcasted_iota(jnp.int32, (HEADS, 128), 0)
    bias = jnp.zeros((HEADS, 128), F32)
    for h in range(HEADS):
        bias = jnp.where(sub == h, bias_ref[h], bias)
    bias = jnp.concatenate([bias] * 8, axis=1)
    position = lax.broadcasted_iota(jnp.int32, (HEADS, CACHE), 1)
    for s in range(SEQ):
        q = qs[pl.ds(s, HEADS, stride=SEQ), :].astype(BF16)
        scores = lax.dot_general(
            q, kc[s], (((1,), (1,)), ((), ())), preferred_element_type=F32
        ) * (HD ** -0.5) + bias
        soft = jnp.log(1.0 + jnp.exp(-jnp.abs(scores)))
        used = position < lengths_ref[s]
        keep = jnp.where(used, -(jnp.maximum(scores, 0.0) + soft), 0.0)
        zs[s] = jnp.where(used, jnp.minimum(scores, 0.0) - soft, -1e30)
        high = keep.astype(BF16)
        rest = (keep - high.astype(F32)).astype(BF16)
        for b in range(4):
            kp[0, s, b] = high[:, b * 256 : (b + 1) * 256]
            kp[1, s, b] = rest[:, b * 256 : (b + 1) * 256]
    col = lax.broadcasted_iota(jnp.int32, (256, 384), 1)
    below = (lax.broadcasted_iota(jnp.int32, (256, 384), 0) > col) | (col >= 256)
    below = jnp.where(below, 1.0, 0.0).astype(BF16)
    loads["value"].wait()
    for s in range(SEQ):
        sums = jnp.dot(kp[0, s].reshape(64, 256), below, preferred_element_type=F32)
        sums = sums + jnp.dot(kp[1, s].reshape(64, 256), below, preferred_element_type=F32)
        carry = jnp.zeros((HEADS, 128), F32)
        parts = [None] * 4
        for b in (3, 2, 1, 0):
            piece = sums[b * 16 : (b + 1) * 16]
            after = piece[:, :256] + jnp.concatenate([carry, carry], axis=1)
            parts[b] = jnp.exp(zs[s, :, b * 256 : (b + 1) * 256] + after).astype(BF16)
            carry = carry + piece[:, 256:]
        weights = jnp.concatenate(parts, axis=1)
        out = jnp.dot(weights, vc[s], preferred_element_type=F32)
        osc[pl.ds(s, HEADS, stride=SEQ), :] = out
    pieces = []
    for j in range(8):
        even, odd = osc[pl.ds(16 * j, 8), :], osc[pl.ds(16 * j + 8, 8), :]
        if j < 4:
            pieces.append(jnp.where(low, even, pltpu.roll(odd, HD, 1)))
        else:
            pieces.append(jnp.where(low, pltpu.roll(even, HD, 1), odd))
    attended = jnp.concatenate(pieces, axis=1).astype(BF16)
    after = hidden
    for i in range(OCHUNK):
        loads[("wo", i)].wait()
        after = after + jnp.dot(
            attended[:, i * orows : (i + 1) * orows], wo[i * orows : (i + 1) * orows, :],
            preferred_element_type=F32,
        )
    after = after.astype(BF16).astype(F32)
    expert_in = rms_norm(after, ffn_gain_ref[...].astype(F32).reshape(1, D)).astype(F32)

    mine = jnp.where(c == 0, expert_in[:, :HALF], expert_in[:, HALF:])
    xin[c] = mine
    xsend[...] = jnp.where(c == 0, expert_in[:, HALF:], expert_in[:, :HALF])
    swap = remote(xsend, xin.at[c], xs_sem, xr_sem, dev(0, 0, 0, 1 - c))
    swap.start()

    loads["wk"].wait()
    loads["wv"].wait()
    newk_ref[...] = jnp.dot(normed, wk[...], preferred_element_type=F32).astype(BF16)
    newv_ref[...] = jnp.dot(normed, wv[...], preferred_element_type=F32).astype(BF16)
    for copy in tcopies:
        copy.wait()

    swap.wait()
    places = jnp.where(table[0].reshape(16, 128) > 0.0, 1.0, 0.0).astype(BF16)
    tokens = xin[...].reshape(16, HALF).astype(BF16)
    packed = lax.dot_general(
        places, tokens, (((0,), (0,)), ((), ())), preferred_element_type=F32
    ).reshape(16, 8, HALF).astype(BF16)
    msg[...] = packed
    blk[0, 0] = packed[0]
    for d in (1, 2, 3, 4, 5, 6, 7, 12, 13, 14, 15, 8, 9, 10, 11):
        remote(
            msg.at[d], blk.at[0, d], d1s, d1r.at[d // 4], dev(d // 4, d % 4, 0, c)
        ).start()

    def rows(g):
        return pl.ds(4 * g, 4)

    def share(k, g):
        copy = remote(blk.at[k, rows(g)], pblk.at[k, rows(g)], ps.at[k, g], pr.at[k, g], dev(0, 0, 0, 1 - c))
        copy.start()
        return copy

    plus, minus, shared, relays = {}, {}, {}, {}
    for g in GROUPS:
        start = 4 * g + (1 if g == 0 else 0)
        drain(blk.at[0, pl.ds(start, 4 * g + 4 - start)], d1r.at[g])
        plus[g] = remote(blk.at[0, rows(g)], blk.at[1, rows(g)], ringp_s.at[g], ringp_r.at[g], dev(0, 0, 1, c))
        plus[g].start()
        minus[g] = remote(blk.at[0, rows(g)], blk.at[2, rows(g)], ringm_s.at[g], ringm_r.at[g], dev(0, 0, 3, c))
        minus[g].start()
        shared[0, g] = share(0, g)

    for name in [("wg", 0), ("wg", 1), ("wu", 0), ("wu", 1), ("wd", 0), ("wd", 1)]:
        loads[name].wait()

    def take(g):
        plus[g].wait_recv()
        shared[1, g] = share(1, g)
        if g in (0, 3):
            relays[g] = remote(blk.at[1, rows(g)], blk.at[3, rows(g)], rel_s.at[g], rel_r.at[g], dev(0, 0, 1, c))
            relays[g].start()
        minus[g].wait_recv()
        shared[2, g] = share(2, g)
        if g in (1, 2):
            relays[g] = remote(blk.at[2, rows(g)], blk.at[3, rows(g)], rel_s.at[g], rel_r.at[g], dev(0, 0, 3, c))
            relays[g].start()

    oshare = {}

    def experts(k):
        for g in GROUPS:
            shared[k, g].wait_recv()
        own, other = blk[k].reshape(128, HALF), pblk[k].reshape(128, HALF)
        gate = jnp.dot(own, wg[0], preferred_element_type=F32) + jnp.dot(other, wg[1], preferred_element_type=F32)
        upper = jnp.dot(own, wu[0], preferred_element_type=F32) + jnp.dot(other, wu[1], preferred_element_type=F32)
        act = (jax.nn.silu(gate) * upper).astype(BF16)
        obuf[k] = jnp.dot(act, wd[1], preferred_element_type=F32).reshape(16, 8, HALF).astype(BF16)
        oshare[k] = remote(obuf.at[k], pout.at[k], os_.at[k], orr.at[k], dev(0, 0, 0, 1 - c))
        oshare[k].start()
        ofull[k] = jnp.dot(act, wd[0], preferred_element_type=F32).reshape(16, 8, HALF)

    def give_back(k):
        oshare[k].wait_recv()
        total = (ofull[k] + pout[k].astype(F32)).astype(BF16)
        rbuf[k] = total
        ybuf[k, 0] = total[0]
        for d in range(1, 16):
            remote(
                rbuf.at[k, d], ybuf.at[k, d], ys.at[k], yr.at[k], dev(4 - d // 4, 4 - d % 4, 0, c)
            ).start()

    take(0)
    experts(0)
    give_back(0)
    take(1)
    take(3)
    take(2)
    experts(1)
    experts(2)
    give_back(1)
    for g in GROUPS:
        relays[g].wait_recv()
        shared[3, g] = share(3, g)
    give_back(2)
    experts(3)
    give_back(3)

    fcopies = []
    for k in range(4):
        drain(ybuf.at[k, pl.ds(1, 15)], yr.at[k])
        scale = table[k].reshape(16, 128).astype(BF16)
        combined = jnp.dot(scale, ybuf[k].reshape(128, HALF), preferred_element_type=F32)
        combined = combined.reshape(2, SEQ, HALF).astype(BF16)
        fsend[k] = combined
        for o in range(2):
            core = (c + o) % 2
            if k == 0 and o == 0:
                fbuf[0, c] = fsend[0, c]
                continue
            copy = remote(
                fsend.at[k, core], fbuf.at[k, c], fs.at[k, o], fr.at[k, o], dev(0, 0, XOFF[k], core)
            )
            copy.start()
            fcopies.append(copy)
    for copy in fcopies:
        copy.wait()
    total = fbuf[0].astype(F32) + fbuf[1].astype(F32) + fbuf[2].astype(F32) + fbuf[3].astype(F32)
    mixed_ref[:, :HALF] = (after[:, :HALF] + total[0]).astype(BF16)
    mixed_ref[:, HALF:] = (after[:, HALF:] + total[1]).astype(BF16)

    drain(msg.at[pl.ds(1, 15)], d1s)
    for g in range(4):
        plus[g].wait_send()
        minus[g].wait_send()
        relays[g].wait_send()
        for k in range(4):
            shared[k, g].wait_send()
    for k in range(4):
        oshare[k].wait_send()
        drain(rbuf.at[k, pl.ds(1, 15)], ys.at[k])


def local(*args):
    vmem = pl.BlockSpec(memory_space=pltpu.VMEM)
    smem = pl.BlockSpec(memory_space=pltpu.SMEM)
    hbm = pl.BlockSpec(memory_space=pl.ANY)
    dma = pltpu.SemaphoreType.DMA
    scratch = [
        pltpu.VMEM((D, HEADS * HD), BF16),
        pltpu.VMEM((D, 128), BF16),
        pltpu.VMEM((D, 128), BF16),
        pltpu.VMEM((SEQ, CACHE, 128), BF16),
        pltpu.VMEM((SEQ, CACHE, 128), BF16),
        pltpu.VMEM((HEADS * HD, D), BF16),
        pltpu.VMEM((2, HALF, FFD), BF16),
        pltpu.VMEM((2, HALF, FFD), BF16),
        pltpu.VMEM((2, FFD, HALF), BF16),
        pltpu.VMEM((128, 128), F32),
        pltpu.VMEM((SEQ, HEADS, CACHE), F32),
        pltpu.VMEM((2, SEQ, 4, HEADS, 256), BF16),
        pltpu.VMEM((128, 128), F32),
        pltpu.VMEM((4, 2, SEQ, 128), F32),
        pltpu.VMEM((2, SEQ, HALF), F32),
        pltpu.VMEM((SEQ, HALF), F32),
        pltpu.VMEM((16, 8, HALF), BF16),
        pltpu.VMEM((4, 16, 8, HALF), BF16),
        pltpu.VMEM((4, 16, 8, HALF), BF16),
        pltpu.VMEM((4, 16, 8, HALF), F32),
        pltpu.VMEM((4, 16, 8, HALF), BF16),
        pltpu.VMEM((4, 16, 8, HALF), BF16),
        pltpu.VMEM((4, 16, 8, HALF), BF16),
        pltpu.VMEM((4, 16, 8, HALF), BF16),
        pltpu.VMEM((4, 2, SEQ, HALF), BF16),
        pltpu.VMEM((4, 2, SEQ, HALF), BF16),
        dma((QCHUNK + OCHUNK + 10,)),
        dma((7,)), dma((7,)),
        dma, dma,
        dma, dma((4,)),
        dma((4,)), dma((4,)),
        dma((4,)), dma((4,)),
        dma((4,)), dma((4,)),
        dma((4, 4)), dma((4, 4)),
        dma((4,)), dma((4,)),
        dma((4,)), dma((4,)),
        dma((4, 2)), dma((4, 2)),
    ]
    return pl.pallas_call(
        kernel,
        out_shape=(
            jax.ShapeDtypeStruct((SEQ, D), BF16),
            jax.ShapeDtypeStruct((SEQ, 128), BF16),
            jax.ShapeDtypeStruct((SEQ, 128), BF16),
        ),
        in_specs=[vmem, smem, hbm, hbm, vmem, hbm, hbm, hbm, smem, hbm, vmem, vmem, vmem, hbm, hbm, hbm],
        out_specs=(vmem, vmem, vmem),
        scratch_shapes=scratch,
        compiler_params=pltpu.CompilerParams(
            collective_id=0, has_side_effects=True, vmem_limit_bytes=60 * 2**20
        ),
        name="layer",
    )(*args)


def solution(mesh):
    ep2, ep3 = P("ep", None), P("ep", None, None)
    in_specs = (ep2, P("ep"), ep3, ep3, P(), P(), P(), P(), P(), P(), P(), ep2, ep2, ep3, ep3, ep3)
    return jax.shard_map(
        local, mesh=mesh, in_specs=in_specs, out_specs=(ep2, ep2, ep2), check_vma=False
    )
```

time: 120 us -> 58.9 us (0.49)
  Pallas kernels: 0 us -> 47.1 us
  blocking collectives: 41.8 us -> 0 us
  waiting for transfers between devices: 26.8 us -> 0 us
  matrix products: 20.3 us -> 0 us
  local copies, waits for them, and re-layouts: 18.4 us -> 10.8 us
  other arithmetic: 7.23 us -> 0 us
  starting transfers between devices: 4.41 us -> 0 us
    pallas_call x0 -> x1, Pallas kernels: none -> 47.1 us  [local(): pl.pallas_call(kernel, out_shape=(jax.ShapeDtypeStruct((SEQ, D), BF16), j...]
    all_to_all x1 -> x0, blocking collectives: 41.8 us -> none  [local(): lax.all_to_all(outgoing, 'ep', split_axis=0, concat_axis=0, tiled=True)]
    all_to_all x1 -> x0, waiting for transfers between devices: 26.8 us -> none  [local(): lax.all_to_all(partial_value.astype(jnp.bfloat16), 'ep', split_axis=0, co...]
    dot_general x14 -> x0, matrix products: 20.3 us -> none  [the longest x1 3.08 us: expert_rows(): gate = jnp.dot(rows, gate_w, preferred_element_type=jnp.float32)]
    all_to_all x1 -> x0, starting transfers between devices: 4.41 us -> none  [local(): lax.all_to_all(partial_value.astype(jnp.bfloat16), 'ep', split_axis=0, co...]
    convert_element_type x4 -> x0, local copies, waits for them, and re-layouts: 4.14 us -> none  [the longest x1 2.97 us: local(): partial_value.astype(jnp.bfloat16)]
    reduce_sum x4 -> x0, other arithmetic: 3.87 us -> none  [the longest x1 1.35 us: local(): table = jnp.sum(picked * route_w.astype(jnp.float32)[:, :, None], axis=1)]
    reshape x3 -> x0, local copies, waits for them, and re-layouts: 3.65 us -> none  [the longest x1 2.06 us: local(): received.reshape(sources * items, width)]
  transfers between devices with their start and end apart: 1 -> 0, of which waited for: 1 -> 0; matrix products, arithmetic and copies ran while one was open for 3% -> 0% of each run, Pallas kernels for 0% -> 0%
where the time goes in v1:
time: 58.9 us; the launch traced here: 58.6 us
  Pallas kernels  47.1 us (80%)
  local copies, waits for them, and re-layouts  10.8 us (18%)
  between operations  0.65 us (1%)
    pallas_call x1, Pallas kernels, local(): pl.pallas_call(kernel, out_shape=(jax.ShapeDtypeStruct((SEQ, D), BF16), j...  47.1 us
    unnamed x9, local copies, waits for them, and re-layouts  10.8 us

profile of v1, /device:TPU:1, one launch (start us, length us, event | category | flops | bytes accessed | tf_op | source)
XLA Modules:
  0.0 58.6 jit_solution(9746658844185253196)
XLA Ops:
  0.6 0.0 copy-start
  0.6 1.4 %copy.20.route_w_ref = bf16[8,2]{1,0:T(8,128)(2,1)} copy(bf16[8,2]{0,1:T(2,128)(2,1)} %param.28) | data formatting | bytes 64 | tf_op args[12]
  2.1 1.3 %copy.19.routing_ref = s32[8,2]{1,0:T(8,128)} copy(s32[8,2]{0,1:T(2,128)} %param.27) | data formatting | bytes 128 | tf_op args[11]
  3.4 2.6 %copy.21.wg_hbm = bf16[1,2048,352]{2,1,0:T(8,128)(2,1)} copy(bf16[1,2048,352]{1,2,0:T(8,128)(2,1)} %param.29) | data formatting | bytes 2883584 | tf_op args[13]
  6.0 0.0 copy-done
  6.0 1.6 %copy.22.wu_hbm = bf16[1,2048,352]{2,1,0:T(8,128)(2,1)} copy(bf16[1,2048,352]{1,2,0:T(8,128)(2,1)S(1)} %copy-done) | data formatting | bytes 2883584 | tf_op args[14]
  7.5 47.1 %layer.1 = (bf16[8,2048]{1,0:T(8,128)(2,1)}, bf16[8,128]{1,0:T(8,128)(2,1)}, bf16[8,128]{1,0:T(8,128)(2,1)}) custom-call(bf16[8,2048]{1,0:T(8,128)(2,1)} %hidden_ref.1, s32[8]{0:T(128)} %lengths_ref.1, bf16[8,1024,128]{2,1,0:T(8,128)(2,1)} %key_hbm.1, bf16[8,1024,128]{2,1,0:T(8,128)(2,1)} %value_hbm.1, bf16[2048]{0:T(1024)(128)(2,1)} %norm_gain_ref.1, ...), custom_call_target="tpu_custom_call" | custom-call | tf_op jit(solution)/shard_map/layer/pallas_call | solution.py:371
  54.7 1.4 %copy.26 = bf16[8,2048]{1,0:T(8,128)(2,1)} copy(bf16[8,2048]{1,0:T(8,128)(2,1)} %get-tuple-element.6) | data formatting | bytes 65536
  56.1 1.3 %copy.27 = bf16[8,128]{1,0:T(8,128)(2,1)} copy(bf16[8,128]{1,0:T(8,128)(2,1)} %get-tuple-element.7) | data formatting | bytes 4096
  57.3 1.2 %copy.28 = bf16[8,128]{1,0:T(8,128)(2,1)} copy(bf16[8,128]{1,0:T(8,128)(2,1)} %get-tuple-element.8) | data formatting | bytes 4096
Async XLA Ops:
  0.6 5.4 %copy-start = (bf16[1,2048,352]{1,2,0:T(8,128)(2,1)S(1)}, bf16[1,2048,352]{1,2,0:T(8,128)(2,1)}, u32[]{:S(2)}) copy-start(bf16[1,2048,352]{1,2,0:T(8,128)(2,1)} %param.30) | copy-start | bytes 4325380

commit v2 on v1

v2 whole, which is shorter than its diff:
```python
import jax
import jax.numpy as jnp
from jax import lax
from jax.experimental import pallas as pl
from jax.experimental.pallas import tpu as pltpu
from jax.sharding import PartitionSpec as P

D = 2048
HEADS = 16
HD = 64
CACHE = 1024
SEQ = 8
FFD = 352
HALF = D // 2
F32 = jnp.float32
BF16 = jnp.bfloat16
MESH = pl.DeviceIdType.MESH
XOFF = (0, 3, 1, 2)
GROUPS = (0, 1, 3, 2)
QCHUNK = 4
OCHUNK = 2


def rms_norm(wide, gain):
    scaled = wide * lax.rsqrt(jnp.mean(wide * wide, axis=-1, keepdims=True) + 1e-06)
    return (scaled * gain).astype(BF16)


def dot_t(a, b):
    return lax.dot_general(a, b, (((1,), (1,)), ((), ())), preferred_element_type=F32)


def kernel(
    hidden_hbm, lengths_ref, key_hbm, value_hbm, norm_gain_hbm, wq_hbm, wk_hbm, wv_hbm, bias_ref,
    wo_hbm, ffn_gain_hbm, routing_hbm, route_w_hbm, wg_hbm, wu_hbm, wd_hbm,
    mixed_hbm, newk_hbm, newv_hbm,
    hidden_ref, norm_gain_ref, ffn_gain_ref, routing_ref, route_w_ref, mixed_ref, newk_ref, newv_ref,
    wq, wkv, kc, vc, wo, wexp,
    qs, zs, kp, sums, osc, table, xin, xsend, msg, blk, pblk, ofull, obuf, pout, rbuf, ybuf, fsend, fbuf,
    lsem, kvsem, esem, tsend, trecv, xs_sem, xr_sem, d1s, d1r, ring_s, ringp_r, ringm_r, rel_s, rel_r,
    ps, pr, os_, orr, ys, yr, fs, fr, outs,
):
    me = lax.axis_index("ep")
    c = me % 2
    x = (me // 2) % 4
    y = (me // 8) % 4
    z = me // 32

    def dev(dz, dy, dx, core):
        return ((((z + dz) % 4) * 4 + (y + dy) % 4) * 4 + (x + dx) % 4) * 2 + core

    def remote(src, dst, ssem, rsem, target):
        return pltpu.make_async_remote_copy(
            src_ref=src, dst_ref=dst, send_sem=ssem, recv_sem=rsem,
            device_id=(target,), device_id_type=MESH,
        )

    def drain(ref, sem):
        pltpu.make_async_copy(ref, ref, sem).wait()

    loads = {}

    def load(name, src, dst, shared=None):
        copy = pltpu.make_async_copy(src, dst, lsem.at[len(loads)] if shared is None else shared)
        copy.start()
        if shared is None:
            loads[name] = copy

    load("hidden", hidden_hbm, hidden_ref)
    load("norm_gain", norm_gain_hbm, norm_gain_ref)
    qrows = D // QCHUNK
    for i in range(QCHUNK):
        load(("wq", i), wq_hbm.at[pl.ds(i * qrows, qrows)], wq.at[pl.ds(i * qrows, qrows)])
    load("key", key_hbm, kc)
    load("value", value_hbm, vc)
    load("routing", routing_hbm, routing_ref)
    load("route_w", route_w_hbm, route_w_ref)
    load("ffn_gain", ffn_gain_hbm, ffn_gain_ref)
    orows = HEADS * HD // OCHUNK
    for i in range(OCHUNK):
        load(("wo", i), wo_hbm.at[pl.ds(i * orows, orows)], wo.at[pl.ds(i * orows, orows)])
    load("wk", wk_hbm, wkv.at[0], kvsem)
    load("wv", wv_hbm, wkv.at[1], kvsem)
    barrier = pltpu.get_barrier_semaphore()
    partners = [dev(d // 4, d % 4, 0, c) for d in range(1, 16)]
    row = [(k, core) for k in range(4) for core in range(2)]
    rowdev = [(k, o) for k in range(4) for o in range(2) if k + o > 0]
    partners += [dev(0, 0, 4 - XOFF[k], (c + o) % 2) for k, o in rowdev]
    for target in partners:
        pl.semaphore_signal(barrier, inc=1, device_id=(target,), device_id_type=MESH)

    loads["hidden"].wait()
    loads["norm_gain"].wait()
    hidden = hidden_ref[...].astype(F32)
    normed = rms_norm(hidden, norm_gain_ref[...].astype(F32).reshape(1, D))
    query = jnp.zeros((SEQ, HEADS * HD), F32)
    for i in range(QCHUNK):
        loads[("wq", i)].wait()
        query = query + jnp.dot(
            normed[:, i * qrows : (i + 1) * qrows], wq[i * qrows : (i + 1) * qrows, :],
            preferred_element_type=F32,
        )
    query = query.astype(BF16).astype(F32)
    low = lax.broadcasted_iota(jnp.int32, (SEQ, 128), 1) < HD
    for j in range(8):
        tile = query[:, j * 128 : (j + 1) * 128]
        swapped = pltpu.roll(tile, HD, 1)
        if j < 4:
            even, odd = jnp.where(low, tile, 0.0), jnp.where(low, swapped, 0.0)
        else:
            even, odd = jnp.where(low, 0.0, swapped), jnp.where(low, 0.0, tile)
        qs[pl.ds(16 * j, 8), :] = even
        qs[pl.ds(16 * j + 8, 8), :] = odd

    loads["key"].wait()
    sub = lax.broadcasted_iota(jnp.int32, (HEADS, 128), 0)
    bias = jnp.zeros((HEADS, 128), F32)
    for h in range(HEADS):
        bias = jnp.where(sub == h, bias_ref[h], bias)
    bias = jnp.concatenate([bias] * 8, axis=1)
    position = lax.broadcasted_iota(jnp.int32, (HEADS, CACHE), 1)
    for s in range(SEQ):
        q = qs[pl.ds(s, HEADS, stride=SEQ), :].astype(BF16)
        scores = lax.dot_general(
            q, kc[s], (((1,), (1,)), ((), ())), preferred_element_type=F32
        ) * (HD ** -0.5) + bias
        soft = jnp.log(1.0 + jnp.exp(-jnp.abs(scores)))
        used = position < lengths_ref[s]
        keep = jnp.where(used, -(jnp.maximum(scores, 0.0) + soft), 0.0)
        zs[s] = jnp.where(used, jnp.minimum(scores, 0.0) - soft, -1e30)
        high = keep.astype(BF16)
        rest = (keep - high.astype(F32)).astype(BF16)
        for b in range(4):
            kp[s, b, :, :256] = high[:, b * 256 : (b + 1) * 256]
            kp[s, b, :, 256:] = rest[:, b * 256 : (b + 1) * 256]
    col = lax.broadcasted_iota(jnp.int32, (512, 384), 1)
    below = (lax.broadcasted_iota(jnp.int32, (512, 384), 0) % 256 > col) | (col >= 256)
    below = jnp.where(below, 1.0, 0.0).astype(BF16)
    sums[...] = jnp.dot(kp[...].reshape(512, 512), below, preferred_element_type=F32)
    loads["value"].wait()
    for s in range(SEQ):
        carry = jnp.zeros((HEADS, 128), F32)
        parts = [None] * 4
        for b in (3, 2, 1, 0):
            piece = sums[pl.ds(s * 64 + b * 16, 16), :]
            after = piece[:, :256] + jnp.concatenate([carry, carry], axis=1)
            parts[b] = jnp.exp(zs[s, :, b * 256 : (b + 1) * 256] + after).astype(BF16)
            carry = carry + piece[:, 256:]
        weights = jnp.concatenate(parts, axis=1)
        out = jnp.dot(weights, vc[s], preferred_element_type=F32)
        osc[pl.ds(s, HEADS, stride=SEQ), :] = out
    pieces = []
    for j in range(8):
        even, odd = osc[pl.ds(16 * j, 8), :], osc[pl.ds(16 * j + 8, 8), :]
        if j < 4:
            pieces.append(jnp.where(low, even, pltpu.roll(odd, HD, 1)))
        else:
            pieces.append(jnp.where(low, pltpu.roll(even, HD, 1), odd))
    attended = jnp.concatenate(pieces, axis=1).astype(BF16)
    after = hidden
    for i in range(OCHUNK):
        loads[("wo", i)].wait()
        after = after + jnp.dot(
            attended[:, i * orows : (i + 1) * orows], wo[i * orows : (i + 1) * orows, :],
            preferred_element_type=F32,
        )
    after = after.astype(BF16).astype(F32)
    loads["ffn_gain"].wait()
    expert_in = rms_norm(after, ffn_gain_ref[...].astype(F32).reshape(1, D)).astype(F32)

    for i in range(2):
        half = (c + i) % 2
        cols = pl.ds(pl.multiple_of(half * HALF, HALF), HALF)
        load("wg", wg_hbm.at[0, :, cols], wexp.at[i], esem)
        load("wu", wu_hbm.at[0, :, cols], wexp.at[2 + i], esem)
        load("wd", wd_hbm.at[0, :, cols], wexp.at[4 + i], esem)

    lane = lax.broadcasted_iota(jnp.int32, (SEQ, 128), 1)
    plane = lane // 8
    lz = (z + plane // 4) % 4
    ly = (y + plane % 4) % 4
    lexpert = 2 * lz + ly // 2
    diagonal = lax.broadcasted_iota(jnp.int32, (SEQ, SEQ), 0) == lax.broadcasted_iota(jnp.int32, (SEQ, SEQ), 1)

    def column(row):
        return jnp.sum(jnp.where(diagonal, row, 0.0), axis=1, keepdims=True)

    loads["routing"].wait()
    loads["route_w"].wait()
    routing = routing_ref[...].astype(F32)
    route_w = route_w_ref[...].astype(F32)
    lexpert = lexpert.astype(F32)
    is_first = jnp.abs(lexpert - column(routing[0:1])) < 0.5
    is_second = jnp.abs(lexpert - column(routing[1:2])) < 0.5
    named = jnp.where(is_first | is_second, 1.0, 0.0).astype(F32)
    tri = (
        lax.broadcasted_iota(jnp.int32, (SEQ, SEQ), 0) >= lax.broadcasted_iota(jnp.int32, (SEQ, SEQ), 1)
    ).astype(F32)
    rank = jnp.dot(tri, named, preferred_element_type=F32)
    here = (jnp.abs(rank - 1.0 - (lane % 4).astype(F32)) < 0.5) & ((lane // 4) % 2 == c)
    weight = jnp.where(is_first, column(route_w[0:1]), jnp.where(is_second, column(route_w[1:2]), 0.0))
    table[c] = jnp.where(here, weight, 0.0)

    pl.semaphore_wait(barrier, len(partners))
    for i, (k, o) in enumerate(rowdev):
        copy = remote(
            table.at[c], table.at[2 * k + c], tsend, trecv.at[min(k, 1)],
            dev(0, 0, 4 - XOFF[k], (c + o) % 2),
        )
        copy.start()

    mine = jnp.where(c == 0, expert_in[:, :HALF], expert_in[:, HALF:])
    xin[c] = mine
    xsend[...] = jnp.where(c == 0, expert_in[:, HALF:], expert_in[:, :HALF])
    swap = remote(xsend, xin.at[c], xs_sem, xr_sem, dev(0, 0, 0, 1 - c))
    swap.start()

    drain(wkv, kvsem)
    newk_ref[...] = jnp.dot(normed, wkv[0], preferred_element_type=F32).astype(BF16)
    newv_ref[...] = jnp.dot(normed, wkv[1], preferred_element_type=F32).astype(BF16)
    out_copies = [
        pltpu.make_async_copy(newk_ref, newk_hbm, outs.at[0]),
        pltpu.make_async_copy(newv_ref, newv_hbm, outs.at[1]),
    ]
    for copy in out_copies:
        copy.start()
    drain(table.at[0], trecv.at[0])

    swap.wait_recv()
    places = jnp.where(table[0:2].reshape(16, 128) > 0.0, 1.0, 0.0).astype(BF16)
    tokens = xin[...].reshape(16, HALF).astype(BF16)
    packed = lax.dot_general(
        places, tokens, (((0,), (0,)), ((), ())), preferred_element_type=F32
    ).reshape(16, 8, HALF).astype(BF16)
    msg[...] = packed
    blk[0, 0] = packed[0]
    for d in (1, 2, 3, 4, 5, 6, 7, 12, 13, 14, 15, 8, 9, 10, 11):
        remote(
            msg.at[d], blk.at[0, d], d1s, d1r.at[d // 4], dev(d // 4, d % 4, 0, c)
        ).start()

    def rows(g):
        return pl.ds(4 * g, 4)

    def share(k, g):
        copy = remote(blk.at[k, rows(g)], pblk.at[k, rows(g)], ps, pr.at[k], dev(0, 0, 0, 1 - c))
        copy.start()

    plus, minus, relays = {}, {}, {}
    for g in GROUPS:
        start = 4 * g + (1 if g == 0 else 0)
        drain(blk.at[0, pl.ds(start, 4 * g + 4 - start)], d1r.at[g])
        plus[g] = remote(blk.at[0, rows(g)], blk.at[1, rows(g)], ring_s, ringp_r.at[g], dev(0, 0, 1, c))
        plus[g].start()
        minus[g] = remote(blk.at[0, rows(g)], blk.at[2, rows(g)], ring_s, ringm_r.at[g], dev(0, 0, 3, c))
        minus[g].start()
        share(0, g)

    drain(wexp, esem)

    def take(g):
        plus[g].wait_recv()
        share(1, g)
        if g in (0, 3):
            relays[g] = remote(blk.at[1, rows(g)], blk.at[3, rows(g)], rel_s, rel_r.at[g], dev(0, 0, 1, c))
            relays[g].start()
        minus[g].wait_recv()
        share(2, g)
        if g in (1, 2):
            relays[g] = remote(blk.at[2, rows(g)], blk.at[3, rows(g)], rel_s, rel_r.at[g], dev(0, 0, 3, c))
            relays[g].start()

    oshare = {}

    def experts(k, count):
        span = pl.ds(k, count)
        own = blk[span].reshape(128 * count, HALF)
        gate, upper = dot_t(wexp[0], own), dot_t(wexp[2], own)
        for j in range(k, k + count):
            drain(pblk.at[j], pr.at[j])
        other = pblk[span].reshape(128 * count, HALF)
        gate, upper = gate + dot_t(wexp[1], other), upper + dot_t(wexp[3], other)
        act = (jax.nn.silu(gate) * upper).T.astype(BF16)
        theirs = jnp.dot(act, wexp[5], preferred_element_type=F32)
        obuf[span] = theirs.reshape(count, 16, 8, HALF).astype(BF16)
        for j in range(k, k + count):
            oshare[j] = remote(obuf.at[j], pout.at[j], os_, orr.at[j], dev(0, 0, 0, 1 - c))
            oshare[j].start()
        ofull[span] = jnp.dot(act, wexp[4], preferred_element_type=F32).reshape(count, 16, 8, HALF)

    def give_back(k):
        oshare[k].wait_recv()
        total = (ofull[k] + pout[k].astype(F32)).astype(BF16)
        rbuf[k] = total
        ybuf[k, 0] = total[0]
        for d in (10, 9, 11, 6, 14, 8, 2, 5, 7, 13, 15, 4, 12, 1, 3):
            remote(
                rbuf.at[k, d], ybuf.at[k, d], ys, yr.at[k], dev(4 - d // 4, 4 - d % 4, 0, c)
            ).start()

    take(0)
    experts(0, 1)
    take(1)
    give_back(0)
    take(3)
    take(2)
    experts(1, 2)
    for g in GROUPS:
        relays[g].wait_recv()
        share(3, g)
    give_back(1)
    give_back(2)
    experts(3, 1)
    give_back(3)

    drain(table.at[pl.ds(2, 6)], trecv.at[1])
    for k in range(4):
        drain(ybuf.at[k, pl.ds(1, 15)], yr.at[k])
        scale = table[2 * k : 2 * k + 2].reshape(16, 128).astype(BF16)
        combined = jnp.dot(scale, ybuf[k].reshape(128, HALF), preferred_element_type=F32)
        combined = combined.reshape(2, SEQ, HALF).astype(BF16)
        for core in range(2):
            fsend[2 * k + core] = combined[core]
        for o in range(2):
            core = (c + o) % 2
            if k == 0 and o == 0:
                fbuf[0, c] = jnp.where(c == 0, combined[0], combined[1])
                continue
            remote(
                fsend.at[2 * k + core], fbuf.at[k, c], fs, fr, dev(0, 0, XOFF[k], core)
            ).start()
    drain(fsend.at[pl.ds(0, 7)], fr)
    total = fbuf[0].astype(F32) + fbuf[1].astype(F32) + fbuf[2].astype(F32) + fbuf[3].astype(F32)
    mixed_ref[:, :HALF] = (after[:, :HALF] + total[0]).astype(BF16)
    mixed_ref[:, HALF:] = (after[:, HALF:] + total[1]).astype(BF16)
    out_copies.append(pltpu.make_async_copy(mixed_ref, mixed_hbm, outs.at[2]))
    out_copies[-1].start()

    drain(fsend.at[pl.ds(0, 7)], fs)
    drain(table.at[pl.ds(0, 7)], tsend)
    swap.wait_send()
    drain(msg.at[pl.ds(1, 15)], d1s)
    drain(blk.at[pl.ds(0, 2)], ring_s)
    drain(blk.at[0], rel_s)
    drain(blk, ps)
    drain(obuf, os_)
    drain(rbuf.at[:, pl.ds(1, 15)], ys)
    for copy in out_copies:
        copy.wait()


def finish(mixed_in, newk_in, newv_in, mixed_ref, newk_ref, newv_ref):
    mixed_ref[...] = mixed_in[...]
    newk_ref[...] = newk_in[...]
    newv_ref[...] = newv_in[...]


def local(*args):
    args = list(args)
    args[11], args[12] = args[11].T, args[12].T
    args[13], args[14] = jnp.swapaxes(args[13], 1, 2), jnp.swapaxes(args[14], 1, 2)
    vmem = pl.BlockSpec(memory_space=pltpu.VMEM)
    smem = pl.BlockSpec(memory_space=pltpu.SMEM)
    hbm = pl.BlockSpec(memory_space=pl.ANY)
    dma = pltpu.SemaphoreType.DMA
    scratch = [
        pltpu.VMEM((SEQ, D), BF16),
        pltpu.VMEM((D,), BF16),
        pltpu.VMEM((D,), BF16),
        pltpu.VMEM((2, SEQ), jnp.int32),
        pltpu.VMEM((2, SEQ), BF16),
        pltpu.VMEM((SEQ, D), BF16),
        pltpu.VMEM((SEQ, 128), BF16),
        pltpu.VMEM((SEQ, 128), BF16),
        pltpu.VMEM((D, HEADS * HD), BF16),
        pltpu.VMEM((2, D, 128), BF16),
        pltpu.VMEM((SEQ, CACHE, 128), BF16),
        pltpu.VMEM((SEQ, CACHE, 128), BF16),
        pltpu.VMEM((HEADS * HD, D), BF16),
        pltpu.VMEM((6, FFD, HALF), BF16),
        pltpu.VMEM((128, 128), F32),
        pltpu.VMEM((SEQ, HEADS, CACHE), F32),
        pltpu.VMEM((SEQ, 4, HEADS, 512), BF16),
        pltpu.VMEM((512, 384), F32),
        pltpu.VMEM((128, 128), F32),
        pltpu.VMEM((8, SEQ, 128), F32),
        pltpu.VMEM((2, SEQ, HALF), F32),
        pltpu.VMEM((SEQ, HALF), F32),
        pltpu.VMEM((16, 8, HALF), BF16),
        pltpu.VMEM((4, 16, 8, HALF), BF16),
        pltpu.VMEM((4, 16, 8, HALF), BF16),
        pltpu.VMEM((4, 16, 8, HALF), F32),
        pltpu.VMEM((4, 16, 8, HALF), BF16),
        pltpu.VMEM((4, 16, 8, HALF), BF16),
        pltpu.VMEM((4, 16, 8, HALF), BF16),
        pltpu.VMEM((4, 16, 8, HALF), BF16),
        pltpu.VMEM((8, SEQ, HALF), BF16),
        pltpu.VMEM((4, 2, SEQ, HALF), BF16),
        dma((QCHUNK + OCHUNK + 7,)), dma, dma,
        dma, dma((2,)),
        dma, dma,
        dma, dma((4,)),
        dma, dma((4,)), dma((4,)),
        dma, dma((4,)),
        dma, dma((4,)),
        dma, dma((4,)),
        dma, dma((4,)),
        dma, dma,
        dma((3,)),
    ]
    out_shape = (
        jax.ShapeDtypeStruct((SEQ, D), BF16),
        jax.ShapeDtypeStruct((SEQ, 128), BF16),
        jax.ShapeDtypeStruct((SEQ, 128), BF16),
    )
    outs = pl.pallas_call(
        kernel,
        out_shape=out_shape,
        in_specs=[hbm, smem, hbm, hbm, hbm, hbm, hbm, hbm, smem, hbm, hbm, hbm, hbm, hbm, hbm, hbm],
        out_specs=(hbm, hbm, hbm),
        scratch_shapes=scratch,
        compiler_params=pltpu.CompilerParams(
            collective_id=0, has_side_effects=True, vmem_limit_bytes=60 * 2**20
        ),
        name="layer",
    )(*args)
    return pl.pallas_call(
        finish, out_shape=out_shape, in_specs=[vmem] * 3, out_specs=(vmem,) * 3, name="finish"
    )(*outs)


def solution(mesh):
    ep2, ep3 = P("ep", None), P("ep", None, None)
    in_specs = (ep2, P("ep"), ep3, ep3, P(), P(), P(), P(), P(), P(), P(), ep2, ep2, ep3, ep3, ep3)
    return jax.shard_map(
        local, mesh=mesh, in_specs=in_specs, out_specs=(ep2, ep2, ep2), check_vma=False
    )
```

time: 58.9 us -> 46.7 us (0.79)
  local copies, waits for them, and re-layouts: 10.8 us -> 0 us
  Pallas kernels: 47.1 us -> 45.8 us
    unnamed x9 -> x0, local copies, waits for them, and re-layouts: 10.8 us -> none
    pallas_call x1 -> x2, Pallas kernels: 47.1 us -> 45.8 us  [the longest x1 44.4 us: local(): pl.pallas_call(kernel, out_shape=out_shape, in_specs=[hbm, smem, hbm, hbm...]
where the time goes in v2:
time: 46.7 us; the launch traced here: 46.5 us
  Pallas kernels  45.8 us (98%)
  between operations  0.65 us (1%)
    pallas_call x1, Pallas kernels, local(): pl.pallas_call(kernel, out_shape=out_shape, in_specs=[hbm, smem, hbm, hbm...  44.4 us
    pallas_call x1, Pallas kernels, local(): pl.pallas_call(finish, out_shape=out_shape, in_specs=[vmem] * 3, out_spec...  1.39 us

profile of v2, /device:TPU:1, one launch (start us, length us, event | category | flops | bytes accessed | tf_op | source)
XLA Modules:
  0.0 46.5 jit_solution(2852036539527549444)
XLA Ops:
  0.6 44.4 %layer.1 = (bf16[8,2048]{1,0:T(8,128)(2,1)}, bf16[8,128]{1,0:T(8,128)(2,1)}, bf16[8,128]{1,0:T(8,128)(2,1)}) custom-call(bf16[8,2048]{1,0:T(8,128)(2,1)} %hidden_hbm.1, s32[8]{0:T(128)} %lengths_ref.1, bf16[8,1024,128]{2,1,0:T(8,128)(2,1)} %key_hbm.1, bf16[8,1024,128]{2,1,0:T(8,128)(2,1)} %value_hbm.1, bf16[2048]{0:T(1024)(128)(2,1)} %norm_gain_hbm.1, ...), custom_call_target="tpu_custom_call" | custom-call | tf_op jit(solution)/shard_map/layer/pallas_call | solution.py:416
  45.1 1.4 %finish.1 = (bf16[8,2048]{1,0:T(8,128)(2,1)}, bf16[8,128]{1,0:T(8,128)(2,1)}, bf16[8,128]{1,0:T(8,128)(2,1)}) custom-call(bf16[8,2048]{1,0:T(8,128)(2,1)} %get-tuple-element.6.mixed_in, bf16[8,128]{1,0:T(8,128)(2,1)} %get-tuple-element.7.newk_in, bf16[8,128]{1,0:T(8,128)(2,1)} %get-tuple-element.8.newv_in), custom_call_target="tpu_custom_call" | custom-call | tf_op jit(solution)/shard_map/finish/pallas_call | solution.py:427

commit v3 on v2

--- a/solution.py
+++ b/solution.py
@@ -12,10 +12,11 @@
 SEQ = 8
 FFD = 352
 HALF = D // 2
+QUART = HALF // 2
 F32 = jnp.float32
 BF16 = jnp.bfloat16
 MESH = pl.DeviceIdType.MESH
-XOFF = (0, 3, 1, 2)
+XOFF = (0, 2, 3, 1)
 GROUPS = (0, 1, 3, 2)
 QCHUNK = 4
 OCHUNK = 2
@@ -33,12 +34,12 @@
 def kernel(
     hidden_hbm, lengths_ref, key_hbm, value_hbm, norm_gain_hbm, wq_hbm, wk_hbm, wv_hbm, bias_ref,
     wo_hbm, ffn_gain_hbm, routing_hbm, route_w_hbm, wg_hbm, wu_hbm, wd_hbm,
-    mixed_hbm, newk_hbm, newv_hbm,
-    hidden_ref, norm_gain_ref, ffn_gain_ref, routing_ref, route_w_ref, mixed_ref, newk_ref, newv_ref,
+    mixed_ref, newk_ref, newv_ref,
+    hidden_ref, norm_gain_ref, ffn_gain_ref, routing_ref, route_w_ref,
     wq, wkv, kc, vc, wo, wexp,
-    qs, zs, kp, sums, osc, table, xin, xsend, msg, blk, pblk, ofull, obuf, pout, rbuf, ybuf, fsend, fbuf,
-    lsem, kvsem, esem, tsend, trecv, xs_sem, xr_sem, d1s, d1r, ring_s, ringp_r, ringm_r, rel_s, rel_r,
-    ps, pr, os_, orr, ys, yr, fs, fr, outs,
+    qs, zs, kp, sums, osc, table, xin, xsend, xfar, msg, msgfar, blk, pblk, ofull, obuf, pout, rbuf, ghold, gbuf, gmsg, ybuf, fsend, fbuf,
+    lsem, kvsem, esem, tsend, trecv, xs_sem, xr_sem, xf_s, xf_r, d1s, d1r, d3s, d3r, ring_s, ringp_r, ringm_r,
+    ps, pr, os_, orr, ys, yls, yr, gs, gr, ygs, ygr, fs, fr, fls, flr, fgs, fgr,
 ):
     me = lax.axis_index("ep")
     c = me % 2
@@ -68,14 +69,14 @@
 
     load("hidden", hidden_hbm, hidden_ref)
     load("norm_gain", norm_gain_hbm, norm_gain_ref)
+    load("routing", routing_hbm, routing_ref)
+    load("route_w", route_w_hbm, route_w_ref)
+    load("ffn_gain", ffn_gain_hbm, ffn_gain_ref)
     qrows = D // QCHUNK
     for i in range(QCHUNK):
         load(("wq", i), wq_hbm.at[pl.ds(i * qrows, qrows)], wq.at[pl.ds(i * qrows, qrows)])
     load("key", key_hbm, kc)
     load("value", value_hbm, vc)
-    load("routing", routing_hbm, routing_ref)
-    load("route_w", route_w_hbm, route_w_ref)
-    load("ffn_gain", ffn_gain_hbm, ffn_gain_ref)
     orows = HEADS * HD // OCHUNK
     for i in range(OCHUNK):
         load(("wo", i), wo_hbm.at[pl.ds(i * orows, orows)], wo.at[pl.ds(i * orows, orows)])
@@ -111,6 +112,32 @@
             even, odd = jnp.where(low, 0.0, swapped), jnp.where(low, 0.0, tile)
         qs[pl.ds(16 * j, 8), :] = even
         qs[pl.ds(16 * j + 8, 8), :] = odd
+
+    lane = lax.broadcasted_iota(jnp.int32, (SEQ, 128), 1)
+    plane = lane // 8
+    lz = (z + plane // 4) % 4
+    ly = (y + plane % 4) % 4
+    lexpert = 2 * lz + ly // 2
+    diagonal = lax.broadcasted_iota(jnp.int32, (SEQ, SEQ), 0) == lax.broadcasted_iota(jnp.int32, (SEQ, SEQ), 1)
+
+    def column(row):
+        return jnp.sum(jnp.where(diagonal, row, 0.0), axis=1, keepdims=True)
+
+    loads["routing"].wait()
+    loads["route_w"].wait()
+    routing = routing_ref[...].astype(F32)
+    route_w = route_w_ref[...].astype(F32)
+    lexpert = lexpert.astype(F32)
+    is_first = jnp.abs(lexpert - column(routing[0:1])) < 0.5
+    is_second = jnp.abs(lexpert - column(routing[1:2])) < 0.5
+    named = jnp.where(is_first | is_second, 1.0, 0.0).astype(F32)
+    tri = (
+        lax.broadcasted_iota(jnp.int32, (SEQ, SEQ), 0) >= lax.broadcasted_iota(jnp.int32, (SEQ, SEQ), 1)
+    ).astype(F32)
+    rank = jnp.dot(tri, named, preferred_element_type=F32)
+    here = (jnp.abs(rank - 1.0 - (lane % 4).astype(F32)) < 0.5) & ((lane // 4) % 2 == c)
+    weight = jnp.where(is_first, column(route_w[0:1]), jnp.where(is_second, column(route_w[1:2]), 0.0))
+    table[c] = jnp.where(here, weight, 0.0)
 
     loads["key"].wait()
     sub = lax.broadcasted_iota(jnp.int32, (HEADS, 128), 0)
@@ -175,69 +202,51 @@
         load("wu", wu_hbm.at[0, :, cols], wexp.at[2 + i], esem)
         load("wd", wd_hbm.at[0, :, cols], wexp.at[4 + i], esem)
 
-    lane = lax.broadcasted_iota(jnp.int32, (SEQ, 128), 1)
-    plane = lane // 8
-    lz = (z + plane // 4) % 4
-    ly = (y + plane % 4) % 4
-    lexpert = 2 * lz + ly // 2
-    diagonal = lax.broadcasted_iota(jnp.int32, (SEQ, SEQ), 0) == lax.broadcasted_iota(jnp.int32, (SEQ, SEQ), 1)
-
-    def column(row):
-        return jnp.sum(jnp.where(diagonal, row, 0.0), axis=1, keepdims=True)
-
-    loads["routing"].wait()
-    loads["route_w"].wait()
-    routing = routing_ref[...].astype(F32)
-    route_w = route_w_ref[...].astype(F32)
-    lexpert = lexpert.astype(F32)
-    is_first = jnp.abs(lexpert - column(routing[0:1])) < 0.5
-    is_second = jnp.abs(lexpert - column(routing[1:2])) < 0.5
-    named = jnp.where(is_first | is_second, 1.0, 0.0).astype(F32)
-    tri = (
-        lax.broadcasted_iota(jnp.int32, (SEQ, SEQ), 0) >= lax.broadcasted_iota(jnp.int32, (SEQ, SEQ), 1)
-    ).astype(F32)
-    rank = jnp.dot(tri, named, preferred_element_type=F32)
-    here = (jnp.abs(rank - 1.0 - (lane % 4).astype(F32)) < 0.5) & ((lane // 4) % 2 == c)
-    weight = jnp.where(is_first, column(route_w[0:1]), jnp.where(is_second, column(route_w[1:2]), 0.0))
-    table[c] = jnp.where(here, weight, 0.0)
-
     pl.semaphore_wait(barrier, len(partners))
     for i, (k, o) in enumerate(rowdev):
         copy = remote(
-            table.at[c], table.at[2 * k + c], tsend, trecv.at[min(k, 1)],
+            table.at[c], table.at[2 * k + c], tsend, trecv.at[(0, 2, 1, 1)[k]],
             dev(0, 0, 4 - XOFF[k], (c + o) % 2),
         )
         copy.start()
 
     mine = jnp.where(c == 0, expert_in[:, :HALF], expert_in[:, HALF:])
-    xin[c] = mine
-    xsend[...] = jnp.where(c == 0, expert_in[:, HALF:], expert_in[:, :HALF])
+    xin[c] = mine.astype(BF16)
+    xsend[...] = jnp.where(c == 0, expert_in[:, HALF:], expert_in[:, :HALF]).astype(BF16)
     swap = remote(xsend, xin.at[c], xs_sem, xr_sem, dev(0, 0, 0, 1 - c))
     swap.start()
+    far = [
+        remote(xin.at[c], xfar.at[c], xf_s.at[0], xf_r.at[0], dev(0, 0, 2, c)),
+        remote(xsend, xfar.at[c], xf_s.at[1], xf_r.at[1], dev(0, 0, 2, 1 - c)),
+    ]
+    for copy in far:
+        copy.start()
 
     drain(wkv, kvsem)
     newk_ref[...] = jnp.dot(normed, wkv[0], preferred_element_type=F32).astype(BF16)
     newv_ref[...] = jnp.dot(normed, wkv[1], preferred_element_type=F32).astype(BF16)
-    out_copies = [
-        pltpu.make_async_copy(newk_ref, newk_hbm, outs.at[0]),
-        pltpu.make_async_copy(newv_ref, newv_hbm, outs.at[1]),
-    ]
-    for copy in out_copies:
-        copy.start()
     drain(table.at[0], trecv.at[0])
 
     swap.wait_recv()
-    places = jnp.where(table[0:2].reshape(16, 128) > 0.0, 1.0, 0.0).astype(BF16)
-    tokens = xin[...].reshape(16, HALF).astype(BF16)
-    packed = lax.dot_general(
-        places, tokens, (((0,), (0,)), ((), ())), preferred_element_type=F32
-    ).reshape(16, 8, HALF).astype(BF16)
-    msg[...] = packed
-    blk[0, 0] = packed[0]
-    for d in (1, 2, 3, 4, 5, 6, 7, 12, 13, 14, 15, 8, 9, 10, 11):
-        remote(
-            msg.at[d], blk.at[0, d], d1s, d1r.at[d // 4], dev(d // 4, d % 4, 0, c)
-        ).start()
+
+    def dispatch(k, tokens_ref, out, ssem, rsem):
+        places = jnp.where(table[2 * k : 2 * k + 2].reshape(16, 128) > 0.0, 1.0, 0.0).astype(BF16)
+        tokens = tokens_ref[...].astype(F32).reshape(16, HALF).astype(BF16)
+        packed = lax.dot_general(
+            places, tokens, (((0,), (0,)), ((), ())), preferred_element_type=F32
+        ).reshape(16, 8, HALF).astype(BF16)
+        out[...] = packed
+        blk[k, 0] = packed[0]
+        for d in (1, 2, 3, 4, 5, 6, 7, 12, 13, 14, 15, 8, 9, 10, 11):
+            remote(
+                out.at[d], blk.at[k, d], ssem, rsem.at[d // 4], dev(d // 4, d % 4, 0, c)
+            ).start()
+
+    dispatch(0, xin, msg, d1s, d1r)
+    drain(table.at[pl.ds(0, 2)], trecv.at[2])
+    for copy in far:
+        copy.wait_recv()
+    dispatch(1, xfar, msgfar, d3s, d3r)
 
     def rows(g):
         return pl.ds(4 * g, 4)
@@ -246,13 +255,16 @@
         copy = remote(blk.at[k, rows(g)], pblk.at[k, rows(g)], ps, pr.at[k], dev(0, 0, 0, 1 - c))
         copy.start()
 
-    plus, minus, relays = {}, {}, {}
+    plus, minus = {}, {}
+    def arrive(k, g, sem):
+        start = 4 * g + (1 if g == 0 else 0)
+        drain(blk.at[k, pl.ds(start, 4 * g + 4 - start)], sem.at[g])
+
     for g in GROUPS:
-        start = 4 * g + (1 if g == 0 else 0)
-        drain(blk.at[0, pl.ds(start, 4 * g + 4 - start)], d1r.at[g])
-        plus[g] = remote(blk.at[0, rows(g)], blk.at[1, rows(g)], ring_s, ringp_r.at[g], dev(0, 0, 1, c))
+        arrive(0, g, d1r)
+        plus[g] = remote(blk.at[0, rows(g)], blk.at[2, rows(g)], ring_s, ringp_r.at[g], dev(0, 0, 1, c))
         plus[g].start()
-        minus[g] = remote(blk.at[0, rows(g)], blk.at[2, rows(g)], ring_s, ringm_r.at[g], dev(0, 0, 3, c))
+        minus[g] = remote(blk.at[0, rows(g)], blk.at[3, rows(g)], ring_s, ringm_r.at[g], dev(0, 0, 3, c))
         minus[g].start()
         share(0, g)
 
@@ -260,15 +272,13 @@
 
     def take(g):
         plus[g].wait_recv()
+        share(2, g)
+        minus[g].wait_recv()
+        share(3, g)
+
+    def take_far(g):
+        arrive(1, g, d3r)
         share(1, g)
-        if g in (0, 3):
-            relays[g] = remote(blk.at[1, rows(g)], blk.at[3, rows(g)], rel_s, rel_r.at[g], dev(0, 0, 1, c))
-            relays[g].start()
-        minus[g].wait_recv()
-        share(2, g)
-        if g in (1, 2):
-            relays[g] = remote(blk.at[2, rows(g)], blk.at[3, rows(g)], rel_s, rel_r.at[g], dev(0, 0, 3, c))
-            relays[g].start()
 
     oshare = {}
 
@@ -288,65 +298,120 @@
             oshare[j].start()
         ofull[span] = jnp.dot(act, wexp[4], preferred_element_type=F32).reshape(count, 16, 8, HALF)
 
+    spread = (10, 9, 11, 6, 14, 8, 2, 5, 7, 13, 15, 4, 12, 1, 3)
+    left, right = pl.ds(0, QUART), pl.ds(QUART, QUART)
+
     def give_back(k):
         oshare[k].wait_recv()
-        total = (ofull[k] + pout[k].astype(F32)).astype(BF16)
-        rbuf[k] = total
-        ybuf[k, 0] = total[0]
-        for d in (10, 9, 11, 6, 14, 8, 2, 5, 7, 13, 15, 4, 12, 1, 3):
+        total = ofull[k] + pout[k].astype(F32)
+        rounded = total.astype(BF16)
+        rbuf[k] = rounded
+        if k == 1:
+            ybuf[k, 0] = rounded[0]
+            for d in spread:
+                remote(
+                    rbuf.at[k, d], ybuf.at[k, d], ys, yr.at[k], dev(4 - d // 4, 4 - d % 4, 0, c)
+                ).start()
+            return
+        if k > 0:
+            for h in (1, 0):
+                part = pl.ds(8 * h, 8)
+                remote(
+                    rbuf.at[k, part, :, right], gbuf.at[k - 2, part], gs, gr.at[h], dev(0, 0, XOFF[k], c)
+                ).start()
+        else:
+            ghold[...] = total[:, :, QUART:]
+        ybuf[k, 0, :, :QUART] = rounded[0, :, :QUART]
+        for d in spread:
             remote(
-                rbuf.at[k, d], ybuf.at[k, d], ys, yr.at[k], dev(4 - d // 4, 4 - d % 4, 0, c)
+                rbuf.at[k, d, :, left], ybuf.at[k, d, :, left], yls, yr.at[k],
+                dev(4 - d // 4, 4 - d % 4, 0, c),
             ).start()
 
+    def merge(h):
+        part = pl.ds(8 * h, 8)
+        drain(gbuf.at[:, part], gr.at[h])
+        total = ghold[part] + gbuf[0, part].astype(F32) + gbuf[1, part].astype(F32)
+        gmsg[part] = total.astype(BF16)
+        if h == 0:
+            ybuf[0, 0, :, QUART:] = total[0].astype(BF16)
+        for d in spread:
+            if d // 8 == h:
+                remote(
+                    gmsg.at[d], ybuf.at[0, d, :, right], ygs, ygr, dev(4 - d // 4, 4 - d % 4, 0, c)
+                ).start()
+
+    take_far(0)
+    take_far(1)
     take(0)
-    experts(0, 1)
+    take_far(3)
+    take_far(2)
     take(1)
-    give_back(0)
+    experts(0, 2)
     take(3)
     take(2)
-    experts(1, 2)
-    for g in GROUPS:
-        relays[g].wait_recv()
-        share(3, g)
+    give_back(0)
     give_back(1)
+    experts(2, 2)
     give_back(2)
-    experts(3, 1)
     give_back(3)
-
-    drain(table.at[pl.ds(2, 6)], trecv.at[1])
-    for k in range(4):
-        drain(ybuf.at[k, pl.ds(1, 15)], yr.at[k])
+    merge(1)
+    merge(0)
+
+    drain(table.at[pl.ds(4, 4)], trecv.at[1])
+    def combine(k, low, high):
         scale = table[2 * k : 2 * k + 2].reshape(16, 128).astype(BF16)
-        combined = jnp.dot(scale, ybuf[k].reshape(128, HALF), preferred_element_type=F32)
-        combined = combined.reshape(2, SEQ, HALF).astype(BF16)
-        for core in range(2):
-            fsend[2 * k + core] = combined[core]
+        sums = jnp.dot(scale, ybuf[k, :, :, low:high].reshape(128, high - low), preferred_element_type=F32)
+        return sums.reshape(2, SEQ, high - low).astype(BF16)
+
+    def deliver(k, o, send, recv, cols):
+        core = (c + o) % 2
+        remote(
+            fsend.at[2 * k + core, :, cols], fbuf.at[k, c, :, cols], send, recv, dev(0, 0, XOFF[k], core)
+        ).start()
+
+    for k in (0, 1, 2, 3):
+        if k == 1:
+            drain(ybuf.at[1, pl.ds(1, 15)], yr.at[1])
+            fsend[2:4] = combine(1, 0, HALF)
+            deliver(1, 0, fs, fr, pl.ds(0, HALF))
+            deliver(1, 1, fs, fr, pl.ds(0, HALF))
+            continue
+        drain(ybuf.at[k, pl.ds(1, 15), :, left], yr.at[k])
+        fsend[2 * k : 2 * k + 2, :, :QUART] = combine(k, 0, QUART)
         for o in range(2):
-            core = (c + o) % 2
-            if k == 0 and o == 0:
-                fbuf[0, c] = jnp.where(c == 0, combined[0], combined[1])
-                continue
-            remote(
-                fsend.at[2 * k + core], fbuf.at[k, c], fs, fr, dev(0, 0, XOFF[k], core)
-            ).start()
-    drain(fsend.at[pl.ds(0, 7)], fr)
-    total = fbuf[0].astype(F32) + fbuf[1].astype(F32) + fbuf[2].astype(F32) + fbuf[3].astype(F32)
+            if k + o > 0:
+                deliver(k, o, fls, flr, left)
+    drain(ybuf.at[0, pl.ds(1, 15), :, right], ygr)
+    fsend[0:2, :, QUART:] = combine(0, QUART, HALF)
+    deliver(0, 1, fgs, fgr, right)
+    fbuf[0, c] = fsend[c]
+    drain(fsend.at[pl.ds(0, 5), :, left], flr)
+    drain(fsend.at[pl.ds(0, 2)], fr)
+    drain(fsend.at[0, :, right], fgr)
+    low = fbuf[0, :, :, :QUART].astype(F32) + fbuf[3, :, :, :QUART].astype(F32)
+    low = low + fbuf[1, :, :, :QUART].astype(F32) + fbuf[2, :, :, :QUART].astype(F32)
+    high = fbuf[0, :, :, QUART:].astype(F32) + fbuf[1, :, :, QUART:].astype(F32)
+    total = jnp.concatenate([low, high], axis=-1)
     mixed_ref[:, :HALF] = (after[:, :HALF] + total[0]).astype(BF16)
     mixed_ref[:, HALF:] = (after[:, HALF:] + total[1]).astype(BF16)
-    out_copies.append(pltpu.make_async_copy(mixed_ref, mixed_hbm, outs.at[2]))
-    out_copies[-1].start()
-
-    drain(fsend.at[pl.ds(0, 7)], fs)
+
+    drain(fsend.at[pl.ds(0, 5), :, left], fls)
+    drain(fsend.at[pl.ds(0, 2)], fs)
+    drain(fsend.at[0, :, right], fgs)
+    drain(rbuf.at[pl.ds(2, 2), :, :, right], gs)
+    drain(rbuf.at[pl.ds(0, 3), pl.ds(1, 15), :, left], yls)
+    drain(gmsg.at[pl.ds(1, 15)], ygs)
     drain(table.at[pl.ds(0, 7)], tsend)
     swap.wait_send()
+    for copy in far:
+        copy.wait_send()
     drain(msg.at[pl.ds(1, 15)], d1s)
     drain(blk.at[pl.ds(0, 2)], ring_s)
-    drain(blk.at[0], rel_s)
+    drain(msgfar.at[pl.ds(1, 15)], d3s)
     drain(blk, ps)
     drain(obuf, os_)
-    drain(rbuf.at[:, pl.ds(1, 15)], ys)
-    for copy in out_copies:
-        copy.wait()
+    drain(rbuf.at[1, pl.ds(1, 15)], ys)
 
 
 def finish(mixed_in, newk_in, newv_in, mixed_ref, newk_ref, newv_ref):
@@ -369,9 +434,6 @@
         pltpu.VMEM((D,), BF16),
         pltpu.VMEM((2, SEQ), jnp.int32),
         pltpu.VMEM((2, SEQ), BF16),
-        pltpu.VMEM((SEQ, D), BF16),
-        pltpu.VMEM((SEQ, 128), BF16),
-        pltpu.VMEM((SEQ, 128), BF16),
         pltpu.VMEM((D, HEADS * HD), BF16),
         pltpu.VMEM((2, D, 128), BF16),
         pltpu.VMEM((SEQ, CACHE, 128), BF16),
@@ -384,8 +446,10 @@
         pltpu.VMEM((512, 384), F32),
         pltpu.VMEM((128, 128), F32),
         pltpu.VMEM((8, SEQ, 128), F32),
-        pltpu.VMEM((2, SEQ, HALF), F32),
-        pltpu.VMEM((SEQ, HALF), F32),
+        pltpu.VMEM((2, SEQ, HALF), BF16),
+        pltpu.VMEM((SEQ, HALF), BF16),
+        pltpu.VMEM((2, SEQ, HALF), BF16),
+        pltpu.VMEM((16, 8, HALF), BF16),
         pltpu.VMEM((16, 8, HALF), BF16),
         pltpu.VMEM((4, 16, 8, HALF), BF16),
         pltpu.VMEM((4, 16, 8, HALF), BF16),
@@ -393,20 +457,25 @@
         pltpu.VMEM((4, 16, 8, HALF), BF16),
         pltpu.VMEM((4, 16, 8, HALF), BF16),
         pltpu.VMEM((4, 16, 8, HALF), BF16),
+        pltpu.VMEM((16, 8, QUART), F32),
+        pltpu.VMEM((2, 16, 8, QUART), BF16),
+        pltpu.VMEM((16, 8, QUART), BF16),
         pltpu.VMEM((4, 16, 8, HALF), BF16),
         pltpu.VMEM((8, SEQ, HALF), BF16),
         pltpu.VMEM((4, 2, SEQ, HALF), BF16),
         dma((QCHUNK + OCHUNK + 7,)), dma, dma,
-        dma, dma((2,)),
+        dma, dma((3,)),
         dma, dma,
+        dma((2,)), dma((2,)),
+        dma, dma((4,)),
         dma, dma((4,)),
         dma, dma((4,)), dma((4,)),
         dma, dma((4,)),
         dma, dma((4,)),
-        dma, dma((4,)),
-        dma, dma((4,)),
+        dma, dma, dma((4,)),
+        dma, dma((2,)),
         dma, dma,
-        dma((3,)),
+        dma, dma, dma, dma, dma, dma,
     ]
     out_shape = (
         jax.ShapeDtypeStruct((SEQ, D), BF16),
@@ -415,9 +484,9 @@
     )
     outs = pl.pallas_call(
         kernel,
-        out_shape=out_shape,
+        out_shape=tuple(pltpu.VMEM(o.shape, o.dtype) for o in out_shape),
         in_specs=[hbm, smem, hbm, hbm, hbm, hbm, hbm, hbm, smem, hbm, hbm, hbm, hbm, hbm, hbm, hbm],
-        out_specs=(hbm, hbm, hbm),
+        out_specs=(vmem, vmem, vmem),
         scratch_shapes=scratch,
         compiler_params=pltpu.CompilerParams(
             collective_id=0, has_side_effects=True, vmem_limit_bytes=60 * 2**20
@@ -426,7 +495,7 @@
     )(*args)
     return pl.pallas_call(
         finish, out_shape=out_shape, in_specs=[vmem] * 3, out_specs=(vmem,) * 3, name="finish"
-    )(*outs)
+    )(*[pltpu.with_memory_space_constraint(o, pltpu.VMEM) for o in outs])
 
 
 def solution(mesh):

time: 46.7 us -> 42.4 us (0.908)
  Pallas kernels: 45.8 us -> 41.6 us
    pallas_call x1, Pallas kernels: 44.4 us -> 41 us  [local(): pl.pallas_call(kernel, out_shape=tuple((pltpu.VMEM(o.shape, o.dtype) for...]
    pallas_call x1, Pallas kernels: 1.39 us -> 0.62 us  [local(): pl.pallas_call(finish, out_shape=out_shape, in_specs=[vmem] * 3, out_spec...]
where the time goes in v3:
time: 42.4 us; the launch traced here: 42.3 us
  Pallas kernels  41.6 us (98%)
  between operations  0.65 us (2%)
    pallas_call x1, Pallas kernels, local(): pl.pallas_call(kernel, out_shape=tuple((pltpu.VMEM(o.shape, o.dtype) for...  41 us

profile of v3, /device:TPU:1, one launch (start us, length us, event | category | flops | bytes accessed | tf_op | source)
XLA Modules:
  0.0 42.3 jit_solution(10494717833601358363)
XLA Ops:
  0.6 41.0 %layer.1 = (bf16[8,2048]{1,0:T(8,128)(2,1)S(1)}, bf16[8,128]{1,0:T(8,128)(2,1)S(1)}, bf16[8,128]{1,0:T(8,128)(2,1)S(1)}) custom-call(bf16[8,2048]{1,0:T(8,128)(2,1)} %hidden_hbm.1, s32[8]{0:T(128)} %lengths_ref.1, bf16[8,1024,128]{2,1,0:T(8,128)(2,1)} %key_hbm.1, bf16[8,1024,128]{2,1,0:T(8,128)(2,1)} %value_hbm.1, bf16[2048]{0:T(1024)(128)(2,1)} %norm_gain_hbm.1, ...), custom_call_target="tpu_custom_call" | custom-call | tf_op jit(solution)/shard_map/layer/pallas_call | solution.py:485
  41.6 0.6 %finish.1 = (bf16[8,2048]{1,0:T(8,128)(2,1)}, bf16[8,128]{1,0:T(8,128)(2,1)}, bf16[8,128]{1,0:T(8,128)(2,1)}) custom-call(bf16[8,2048]{1,0:T(8,128)(2,1)S(1)} %get-tuple-element.6.mixed_in, bf16[8,128]{1,0:T(8,128)(2,1)S(1)} %get-tuple-element.7.newk_in, bf16[8,128]{1,0:T(8,128)(2,1)S(1)} %get-tuple-element.8.newv_in), custom_call_target="tpu_custom_call" | custom-call | tf_op jit(solution)/shard_map/finish/pallas_call | solution.py:496

commit v4 on v3

--- a/solution.py
+++ b/solution.py
@@ -12,7 +12,8 @@
 SEQ = 8
 FFD = 352
 HALF = D // 2
-QUART = HALF // 2
+LEFT = 512
+RIGHT = HALF - LEFT
 F32 = jnp.float32
 BF16 = jnp.bfloat16
 MESH = pl.DeviceIdType.MESH
@@ -39,7 +40,7 @@
     wq, wkv, kc, vc, wo, wexp,
     qs, zs, kp, sums, osc, table, xin, xsend, xfar, msg, msgfar, blk, pblk, ofull, obuf, pout, rbuf, ghold, gbuf, gmsg, ybuf, fsend, fbuf,
     lsem, kvsem, esem, tsend, trecv, xs_sem, xr_sem, xf_s, xf_r, d1s, d1r, d3s, d3r, ring_s, ringp_r, ringm_r,
-    ps, pr, os_, orr, ys, yls, yr, gs, gr, ygs, ygr, fs, fr, fls, flr, fgs, fgr,
+    ps, pr, os_, orr, orh, ys, yls, yr, gs, gr, ygs, ygr, fs, fr, fls, flr, fgs, fgr,
 ):
     me = lax.axis_index("ep")
     c = me % 2
@@ -243,46 +244,47 @@
             ).start()
 
     dispatch(0, xin, msg, d1s, d1r)
+    def share(k, part):
+        remote(blk.at[k, part], pblk.at[k, part], ps, pr.at[k], dev(0, 0, 0, 1 - c)).start()
+
+    def rows(g, start=0):
+        return pl.ds(4 * g + start, 4 - start)
+
+    def round_ring(g, part):
+        remote(blk.at[0, part], blk.at[2, part], ring_s, ringp_r.at[g], dev(0, 0, 1, c)).start()
+        remote(blk.at[0, part], blk.at[3, part], ring_s, ringm_r.at[g], dev(0, 0, 3, c)).start()
+        share(0, part)
+
+    round_ring(0, pl.ds(0, 1))
     drain(table.at[pl.ds(0, 2)], trecv.at[2])
     for copy in far:
         copy.wait_recv()
     dispatch(1, xfar, msgfar, d3s, d3r)
 
-    def rows(g):
-        return pl.ds(4 * g, 4)
-
-    def share(k, g):
-        copy = remote(blk.at[k, rows(g)], pblk.at[k, rows(g)], ps, pr.at[k], dev(0, 0, 0, 1 - c))
-        copy.start()
-
-    plus, minus = {}, {}
     def arrive(k, g, sem):
         start = 4 * g + (1 if g == 0 else 0)
         drain(blk.at[k, pl.ds(start, 4 * g + 4 - start)], sem.at[g])
 
     for g in GROUPS:
         arrive(0, g, d1r)
-        plus[g] = remote(blk.at[0, rows(g)], blk.at[2, rows(g)], ring_s, ringp_r.at[g], dev(0, 0, 1, c))
-        plus[g].start()
-        minus[g] = remote(blk.at[0, rows(g)], blk.at[3, rows(g)], ring_s, ringm_r.at[g], dev(0, 0, 3, c))
-        minus[g].start()
-        share(0, g)
+        round_ring(g, rows(g, 1 if g == 0 else 0))
 
     drain(wexp, esem)
 
     def take(g):
-        plus[g].wait_recv()
-        share(2, g)
-        minus[g].wait_recv()
-        share(3, g)
+        drain(blk.at[2, rows(g)], ringp_r.at[g])
+        share(2, rows(g))
+        drain(blk.at[3, rows(g)], ringm_r.at[g])
+        share(3, rows(g))
 
     def take_far(g):
         arrive(1, g, d3r)
-        share(1, g)
-
-    oshare = {}
-
-    def experts(k, count):
+        share(1, rows(g))
+
+    spread = (10, 9, 11, 6, 14, 8, 2, 5, 7, 13, 15, 4, 12, 1, 3)
+    left, right = pl.ds(0, LEFT), pl.ds(LEFT, RIGHT)
+
+    def experts(k, count, between=()):
         span = pl.ds(k, count)
         own = blk[span].reshape(128 * count, HALF)
         gate, upper = dot_t(wexp[0], own), dot_t(wexp[2], own)
@@ -291,52 +293,54 @@
         other = pblk[span].reshape(128 * count, HALF)
         gate, upper = gate + dot_t(wexp[1], other), upper + dot_t(wexp[3], other)
         act = (jax.nn.silu(gate) * upper).T.astype(BF16)
-        theirs = jnp.dot(act, wexp[5], preferred_element_type=F32)
-        obuf[span] = theirs.reshape(count, 16, 8, HALF).astype(BF16)
-        for j in range(k, k + count):
-            oshare[j] = remote(obuf.at[j], pout.at[j], os_, orr.at[j], dev(0, 0, 0, 1 - c))
-            oshare[j].start()
+        for g in between:
+            take(g)
+        for cols, low, high, recv in ((right, LEFT, HALF, orh), (left, 0, LEFT, orr)):
+            theirs = jnp.dot(act, wexp[5, :, low:high], preferred_element_type=F32)
+            obuf[span, :, :, low:high] = theirs.reshape(count, 16, 8, high - low).astype(BF16)
+            for j in range(k, k + count):
+                remote(
+                    obuf.at[j, :, :, cols], pout.at[j, :, :, cols], os_, recv.at[j], dev(0, 0, 0, 1 - c)
+                ).start()
         ofull[span] = jnp.dot(act, wexp[4], preferred_element_type=F32).reshape(count, 16, 8, HALF)
 
-    spread = (10, 9, 11, 6, 14, 8, 2, 5, 7, 13, 15, 4, 12, 1, 3)
-    left, right = pl.ds(0, QUART), pl.ds(QUART, QUART)
+    def send_along(k):
+        drain(pout.at[k, :, :, right], orh.at[k])
+        total = ofull[k, :, :, LEFT:] + pout[k, :, :, LEFT:].astype(F32)
+        if k == 0:
+            ghold[...] = total
+            return
+        rbuf[k, :, :, LEFT:] = total.astype(BF16)
+        for h in (2, 3, 1, 0):
+            part = pl.ds(4 * h, 4)
+            remote(
+                rbuf.at[k, part, :, right], gbuf.at[k - 2, part], gs, gr.at[h], dev(0, 0, XOFF[k], c)
+            ).start()
 
     def give_back(k):
-        oshare[k].wait_recv()
-        total = ofull[k] + pout[k].astype(F32)
-        rounded = total.astype(BF16)
-        rbuf[k] = rounded
         if k == 1:
-            ybuf[k, 0] = rounded[0]
-            for d in spread:
-                remote(
-                    rbuf.at[k, d], ybuf.at[k, d], ys, yr.at[k], dev(4 - d // 4, 4 - d % 4, 0, c)
-                ).start()
-            return
-        if k > 0:
-            for h in (1, 0):
-                part = pl.ds(8 * h, 8)
-                remote(
-                    rbuf.at[k, part, :, right], gbuf.at[k - 2, part], gs, gr.at[h], dev(0, 0, XOFF[k], c)
-                ).start()
-        else:
-            ghold[...] = total[:, :, QUART:]
-        ybuf[k, 0, :, :QUART] = rounded[0, :, :QUART]
+            drain(pout.at[k, :, :, right], orh.at[k])
+        drain(pout.at[k, :, :, left], orr.at[k])
+        high = HALF if k == 1 else LEFT
+        cols = pl.ds(0, high)
+        total = (ofull[k, :, :, :high] + pout[k, :, :, :high].astype(F32)).astype(BF16)
+        rbuf[k, :, :, :high] = total
+        ybuf[k, 0, :, :high] = total[0]
         for d in spread:
             remote(
-                rbuf.at[k, d, :, left], ybuf.at[k, d, :, left], yls, yr.at[k],
+                rbuf.at[k, d, :, cols], ybuf.at[k, d, :, cols], ys if k == 1 else yls, yr.at[k],
                 dev(4 - d // 4, 4 - d % 4, 0, c),
             ).start()
 
     def merge(h):
-        part = pl.ds(8 * h, 8)
+        part = pl.ds(4 * h, 4)
         drain(gbuf.at[:, part], gr.at[h])
         total = ghold[part] + gbuf[0, part].astype(F32) + gbuf[1, part].astype(F32)
         gmsg[part] = total.astype(BF16)
         if h == 0:
-            ybuf[0, 0, :, QUART:] = total[0].astype(BF16)
+            ybuf[0, 0, :, LEFT:] = total[0].astype(BF16)
         for d in spread:
-            if d // 8 == h:
+            if d // 4 == h:
                 remote(
                     gmsg.at[d], ybuf.at[0, d, :, right], ygs, ygr, dev(4 - d // 4, 4 - d % 4, 0, c)
                 ).start()
@@ -352,9 +356,14 @@
     take(2)
     give_back(0)
     give_back(1)
+    send_along(0)
     experts(2, 2)
+    send_along(2)
+    send_along(3)
     give_back(2)
     give_back(3)
+    merge(3)
+    merge(2)
     merge(1)
     merge(0)
 
@@ -378,20 +387,20 @@
             deliver(1, 1, fs, fr, pl.ds(0, HALF))
             continue
         drain(ybuf.at[k, pl.ds(1, 15), :, left], yr.at[k])
-        fsend[2 * k : 2 * k + 2, :, :QUART] = combine(k, 0, QUART)
+        fsend[2 * k : 2 * k + 2, :, :LEFT] = combine(k, 0, LEFT)
         for o in range(2):
             if k + o > 0:
                 deliver(k, o, fls, flr, left)
     drain(ybuf.at[0, pl.ds(1, 15), :, right], ygr)
-    fsend[0:2, :, QUART:] = combine(0, QUART, HALF)
+    fsend[0:2, :, LEFT:] = combine(0, LEFT, HALF)
     deliver(0, 1, fgs, fgr, right)
     fbuf[0, c] = fsend[c]
     drain(fsend.at[pl.ds(0, 5), :, left], flr)
     drain(fsend.at[pl.ds(0, 2)], fr)
     drain(fsend.at[0, :, right], fgr)
-    low = fbuf[0, :, :, :QUART].astype(F32) + fbuf[3, :, :, :QUART].astype(F32)
-    low = low + fbuf[1, :, :, :QUART].astype(F32) + fbuf[2, :, :, :QUART].astype(F32)
-    high = fbuf[0, :, :, QUART:].astype(F32) + fbuf[1, :, :, QUART:].astype(F32)
+    low = fbuf[0, :, :, :LEFT].astype(F32) + fbuf[3, :, :, :LEFT].astype(F32)
+    low = low + fbuf[1, :, :, :LEFT].astype(F32) + fbuf[2, :, :, :LEFT].astype(F32)
+    high = fbuf[0, :, :, LEFT:].astype(F32) + fbuf[1, :, :, LEFT:].astype(F32)
     total = jnp.concatenate([low, high], axis=-1)
     mixed_ref[:, :HALF] = (after[:, :HALF] + total[0]).astype(BF16)
     mixed_ref[:, HALF:] = (after[:, HALF:] + total[1]).astype(BF16)
@@ -457,9 +466,9 @@
         pltpu.VMEM((4, 16, 8, HALF), BF16),
         pltpu.VMEM((4, 16, 8, HALF), BF16),
         pltpu.VMEM((4, 16, 8, HALF), BF16),
-        pltpu.VMEM((16, 8, QUART), F32),
-        pltpu.VMEM((2, 16, 8, QUART), BF16),
-        pltpu.VMEM((16, 8, QUART), BF16),
+        pltpu.VMEM((16, 8, RIGHT), F32),
+        pltpu.VMEM((2, 16, 8, RIGHT), BF16),
+        pltpu.VMEM((16, 8, RIGHT), BF16),
         pltpu.VMEM((4, 16, 8, HALF), BF16),
         pltpu.VMEM((8, SEQ, HALF), BF16),
         pltpu.VMEM((4, 2, SEQ, HALF), BF16),
@@ -471,9 +480,9 @@
         dma, dma((4,)),
         dma, dma((4,)), dma((4,)),
         dma, dma((4,)),
+        dma, dma((4,)), dma((4,)),
+        dma, dma, dma((4,)),
         dma, dma((4,)),
-        dma, dma, dma((4,)),
-        dma, dma((2,)),
         dma, dma,
         dma, dma, dma, dma, dma, dma,
     ]

time: 42.4 us -> 41.3 us (0.974)
  Pallas kernels: 41.6 us -> 40.6 us
    pallas_call x1, Pallas kernels: 41 us -> 40 us  [local(): pl.pallas_call(kernel, out_shape=tuple((pltpu.VMEM(o.shape, o.dtype) for...]
where the time goes in v4:
time: 41.3 us; the launch traced here: 41.2 us
  Pallas kernels  40.6 us (98%)
  between operations  0.65 us (2%)
    pallas_call x1, Pallas kernels, local(): pl.pallas_call(kernel, out_shape=tuple((pltpu.VMEM(o.shape, o.dtype) for...  40 us

profile of v4, /device:TPU:1, one launch (start us, length us, event | category | flops | bytes accessed | tf_op | source)
XLA Modules:
  0.0 41.2 jit_solution(8799931525351489312)
XLA Ops:
  0.6 40.0 %layer.1 = (bf16[8,2048]{1,0:T(8,128)(2,1)S(1)}, bf16[8,128]{1,0:T(8,128)(2,1)S(1)}, bf16[8,128]{1,0:T(8,128)(2,1)S(1)}) custom-call(bf16[8,2048]{1,0:T(8,128)(2,1)} %hidden_hbm.1, s32[8]{0:T(128)} %lengths_ref.1, bf16[8,1024,128]{2,1,0:T(8,128)(2,1)} %key_hbm.1, bf16[8,1024,128]{2,1,0:T(8,128)(2,1)} %value_hbm.1, bf16[2048]{0:T(1024)(128)(2,1)} %norm_gain_hbm.1, ...), custom_call_target="tpu_custom_call" | custom-call | tf_op jit(solution)/shard_map/layer/pallas_call | solution.py:494
  40.6 0.6 %finish.1 = (bf16[8,2048]{1,0:T(8,128)(2,1)}, bf16[8,128]{1,0:T(8,128)(2,1)}, bf16[8,128]{1,0:T(8,128)(2,1)}) custom-call(bf16[8,2048]{1,0:T(8,128)(2,1)S(1)} %get-tuple-element.6.mixed_in, bf16[8,128]{1,0:T(8,128)(2,1)S(1)} %get-tuple-element.7.newk_in, bf16[8,128]{1,0:T(8,128)(2,1)S(1)} %get-tuple-element.8.newv_in), custom_call_target="tpu_custom_call" | custom-call | tf_op jit(solution)/shard_map/finish/pallas_call | solution.py:505

commit v5 on v4

--- a/solution.py
+++ b/solution.py
@@ -33,10 +33,10 @@
 
 
 def kernel(
-    hidden_hbm, lengths_ref, key_hbm, value_hbm, norm_gain_hbm, wq_hbm, wk_hbm, wv_hbm, bias_ref,
+    hidden_hbm, lengths_hbm, key_hbm, value_hbm, norm_gain_hbm, wq_hbm, wk_hbm, wv_hbm, bias_hbm,
     wo_hbm, ffn_gain_hbm, routing_hbm, route_w_hbm, wg_hbm, wu_hbm, wd_hbm,
     mixed_ref, newk_ref, newv_ref,
-    hidden_ref, norm_gain_ref, ffn_gain_ref, routing_ref, route_w_ref,
+    lengths_ref, bias_ref, hidden_ref, norm_gain_ref, ffn_gain_ref, routing_ref, route_w_ref,
     wq, wkv, kc, vc, wo, wexp,
     qs, zs, kp, sums, osc, table, xin, xsend, xfar, msg, msgfar, blk, pblk, ofull, obuf, pout, rbuf, ghold, gbuf, gmsg, ybuf, fsend, fbuf,
     lsem, kvsem, esem, tsend, trecv, xs_sem, xr_sem, xf_s, xf_r, d1s, d1r, d3s, d3r, ring_s, ringp_r, ringm_r,
@@ -70,6 +70,8 @@
 
     load("hidden", hidden_hbm, hidden_ref)
     load("norm_gain", norm_gain_hbm, norm_gain_ref)
+    load("lengths", lengths_hbm, lengths_ref)
+    load("bias", bias_hbm, bias_ref)
     load("routing", routing_hbm, routing_ref)
     load("route_w", route_w_hbm, route_w_ref)
     load("ffn_gain", ffn_gain_hbm, ffn_gain_ref)
@@ -141,6 +143,8 @@
     table[c] = jnp.where(here, weight, 0.0)
 
     loads["key"].wait()
+    loads["lengths"].wait()
+    loads["bias"].wait()
     sub = lax.broadcasted_iota(jnp.int32, (HEADS, 128), 0)
     bias = jnp.zeros((HEADS, 128), F32)
     for h in range(HEADS):
@@ -293,8 +297,8 @@
         other = pblk[span].reshape(128 * count, HALF)
         gate, upper = gate + dot_t(wexp[1], other), upper + dot_t(wexp[3], other)
         act = (jax.nn.silu(gate) * upper).T.astype(BF16)
-        for g in between:
-            take(g)
+        for step, g in between:
+            step(g)
         for cols, low, high, recv in ((right, LEFT, HALF, orh), (left, 0, LEFT, orr)):
             theirs = jnp.dot(act, wexp[5, :, low:high], preferred_element_type=F32)
             obuf[span, :, :, low:high] = theirs.reshape(count, 16, 8, high - low).astype(BF16)
@@ -346,17 +350,17 @@
                 ).start()
 
     take_far(0)
-    take_far(1)
+    experts(0, 1, ((take_far, 1),))
     take(0)
     take_far(3)
     take_far(2)
     take(1)
-    experts(0, 2)
+    give_back(0)
+    send_along(0)
+    experts(1, 1)
     take(3)
     take(2)
-    give_back(0)
     give_back(1)
-    send_along(0)
     experts(2, 2)
     send_along(2)
     send_along(3)
@@ -434,10 +438,11 @@
     args[11], args[12] = args[11].T, args[12].T
     args[13], args[14] = jnp.swapaxes(args[13], 1, 2), jnp.swapaxes(args[14], 1, 2)
     vmem = pl.BlockSpec(memory_space=pltpu.VMEM)
-    smem = pl.BlockSpec(memory_space=pltpu.SMEM)
     hbm = pl.BlockSpec(memory_space=pl.ANY)
     dma = pltpu.SemaphoreType.DMA
     scratch = [
+        pltpu.SMEM((SEQ,), jnp.int32),
+        pltpu.SMEM((HEADS,), F32),
         pltpu.VMEM((SEQ, D), BF16),
         pltpu.VMEM((D,), BF16),
         pltpu.VMEM((D,), BF16),
@@ -472,7 +477,7 @@
         pltpu.VMEM((4, 16, 8, HALF), BF16),
         pltpu.VMEM((8, SEQ, HALF), BF16),
         pltpu.VMEM((4, 2, SEQ, HALF), BF16),
-        dma((QCHUNK + OCHUNK + 7,)), dma, dma,
+        dma((QCHUNK + OCHUNK + 9,)), dma, dma,
         dma, dma((3,)),
         dma, dma,
         dma((2,)), dma((2,)),
@@ -494,7 +499,7 @@
     outs = pl.pallas_call(
         kernel,
         out_shape=tuple(pltpu.VMEM(o.shape, o.dtype) for o in out_shape),
-        in_specs=[hbm, smem, hbm, hbm, hbm, hbm, hbm, hbm, smem, hbm, hbm, hbm, hbm, hbm, hbm, hbm],
+        in_specs=[hbm] * 16,
         out_specs=(vmem, vmem, vmem),
         scratch_shapes=scratch,
         compiler_params=pltpu.CompilerParams(

time: 41.3 us -> 40.6 us (0.983)
  Pallas kernels: 40.6 us -> 39.8 us
    pallas_call x1, Pallas kernels: 40 us -> 39.2 us  [local(): pl.pallas_call(kernel, out_shape=tuple((pltpu.VMEM(o.shape, o.dtype) for...]
where the time goes in v5:
time: 40.6 us; the launch traced here: 40.5 us
  Pallas kernels  39.8 us (98%)
  between operations  0.65 us (2%)
    pallas_call x1, Pallas kernels, local(): pl.pallas_call(kernel, out_shape=tuple((pltpu.VMEM(o.shape, o.dtype) for...  39.2 us

profile of v5, /device:TPU:1, one launch (start us, length us, event | category | flops | bytes accessed | tf_op | source)
XLA Modules:
  0.0 40.5 jit_solution(1449264707474227751)
XLA Ops:
  0.6 39.2 %layer.1 = (bf16[8,2048]{1,0:T(8,128)(2,1)S(1)}, bf16[8,128]{1,0:T(8,128)(2,1)S(1)}, bf16[8,128]{1,0:T(8,128)(2,1)S(1)}) custom-call(bf16[8,2048]{1,0:T(8,128)(2,1)} %hidden_hbm.1, s32[8]{0:T(128)} %lengths_hbm.1, bf16[8,1024,128]{2,1,0:T(8,128)(2,1)} %key_hbm.1, bf16[8,1024,128]{2,1,0:T(8,128)(2,1)} %value_hbm.1, bf16[2048]{0:T(1024)(128)(2,1)} %norm_gain_hbm.1, ...), custom_call_target="tpu_custom_call" | custom-call | tf_op jit(solution)/shard_map/layer/pallas_call | solution.py:499
  39.8 0.6 %finish.1 = (bf16[8,2048]{1,0:T(8,128)(2,1)}, bf16[8,128]{1,0:T(8,128)(2,1)}, bf16[8,128]{1,0:T(8,128)(2,1)}) custom-call(bf16[8,2048]{1,0:T(8,128)(2,1)S(1)} %get-tuple-element.6.mixed_in, bf16[8,128]{1,0:T(8,128)(2,1)S(1)} %get-tuple-element.7.newk_in, bf16[8,128]{1,0:T(8,128)(2,1)S(1)} %get-tuple-element.8.newv_in), custom_call_target="tpu_custom_call" | custom-call | tf_op jit(solution)/shard_map/finish/pallas_call | solution.py:510

commit v6 on v5

--- a/solution.py
+++ b/solution.py
@@ -12,7 +12,7 @@
 SEQ = 8
 FFD = 352
 HALF = D // 2
-LEFT = 512
+LEFT = 640
 RIGHT = HALF - LEFT
 F32 = jnp.float32
 BF16 = jnp.bfloat16
@@ -97,6 +97,32 @@
     loads["norm_gain"].wait()
     hidden = hidden_ref[...].astype(F32)
     normed = rms_norm(hidden, norm_gain_ref[...].astype(F32).reshape(1, D))
+    lane = lax.broadcasted_iota(jnp.int32, (SEQ, 128), 1)
+    plane = lane // 8
+    lz = (z + plane // 4) % 4
+    ly = (y + plane % 4) % 4
+    lexpert = 2 * lz + ly // 2
+    diagonal = lax.broadcasted_iota(jnp.int32, (SEQ, SEQ), 0) == lax.broadcasted_iota(jnp.int32, (SEQ, SEQ), 1)
+
+    def column(row):
+        return jnp.sum(jnp.where(diagonal, row, 0.0), axis=1, keepdims=True)
+
+    loads["routing"].wait()
+    loads["route_w"].wait()
+    routing = routing_ref[...].astype(F32)
+    route_w = route_w_ref[...].astype(F32)
+    lexpert = lexpert.astype(F32)
+    is_first = jnp.abs(lexpert - column(routing[0:1])) < 0.5
+    is_second = jnp.abs(lexpert - column(routing[1:2])) < 0.5
+    named = jnp.where(is_first | is_second, 1.0, 0.0).astype(F32)
+    tri = (
+        lax.broadcasted_iota(jnp.int32, (SEQ, SEQ), 0) >= lax.broadcasted_iota(jnp.int32, (SEQ, SEQ), 1)
+    ).astype(F32)
+    rank = jnp.dot(tri, named, preferred_element_type=F32)
+    here = (jnp.abs(rank - 1.0 - (lane % 4).astype(F32)) < 0.5) & ((lane // 4) % 2 == c)
+    weight = jnp.where(is_first, column(route_w[0:1]), jnp.where(is_second, column(route_w[1:2]), 0.0))
+    table[c] = jnp.where(here, weight, 0.0)
+
     query = jnp.zeros((SEQ, HEADS * HD), F32)
     for i in range(QCHUNK):
         loads[("wq", i)].wait()
@@ -115,32 +141,6 @@
             even, odd = jnp.where(low, 0.0, swapped), jnp.where(low, 0.0, tile)
         qs[pl.ds(16 * j, 8), :] = even
         qs[pl.ds(16 * j + 8, 8), :] = odd
-
-    lane = lax.broadcasted_iota(jnp.int32, (SEQ, 128), 1)
-    plane = lane // 8
-    lz = (z + plane // 4) % 4
-    ly = (y + plane % 4) % 4
-    lexpert = 2 * lz + ly // 2
-    diagonal = lax.broadcasted_iota(jnp.int32, (SEQ, SEQ), 0) == lax.broadcasted_iota(jnp.int32, (SEQ, SEQ), 1)
-
-    def column(row):
-        return jnp.sum(jnp.where(diagonal, row, 0.0), axis=1, keepdims=True)
-
-    loads["routing"].wait()
-    loads["route_w"].wait()
-    routing = routing_ref[...].astype(F32)
-    route_w = route_w_ref[...].astype(F32)
-    lexpert = lexpert.astype(F32)
-    is_first = jnp.abs(lexpert - column(routing[0:1])) < 0.5
-    is_second = jnp.abs(lexpert - column(routing[1:2])) < 0.5
-    named = jnp.where(is_first | is_second, 1.0, 0.0).astype(F32)
-    tri = (
-        lax.broadcasted_iota(jnp.int32, (SEQ, SEQ), 0) >= lax.broadcasted_iota(jnp.int32, (SEQ, SEQ), 1)
-    ).astype(F32)
-    rank = jnp.dot(tri, named, preferred_element_type=F32)
-    here = (jnp.abs(rank - 1.0 - (lane % 4).astype(F32)) < 0.5) & ((lane // 4) % 2 == c)
-    weight = jnp.where(is_first, column(route_w[0:1]), jnp.where(is_second, column(route_w[1:2]), 0.0))
-    table[c] = jnp.where(here, weight, 0.0)
 
     loads["key"].wait()
     loads["lengths"].wait()

time: 40.6 us -> 40.6 us (level)
  no operation moved by 1% of the time
where the time goes in v6:
time: 40.6 us; the launch traced here: 40.4 us
  Pallas kernels  39.8 us (98%)
  between operations  0.65 us (2%)
    pallas_call x1, Pallas kernels, local(): pl.pallas_call(kernel, out_shape=tuple((pltpu.VMEM(o.shape, o.dtype) for...  39.2 us

profile of v6, /device:TPU:1, one launch (start us, length us, event | category | flops | bytes accessed | tf_op | source)
XLA Modules:
  0.0 40.4 jit_solution(14693826931693298445)
XLA Ops:
  0.6 39.2 %layer.1 = (bf16[8,2048]{1,0:T(8,128)(2,1)S(1)}, bf16[8,128]{1,0:T(8,128)(2,1)S(1)}, bf16[8,128]{1,0:T(8,128)(2,1)S(1)}) custom-call(bf16[8,2048]{1,0:T(8,128)(2,1)} %hidden_hbm.1, s32[8]{0:T(128)} %lengths_hbm.1, bf16[8,1024,128]{2,1,0:T(8,128)(2,1)} %key_hbm.1, bf16[8,1024,128]{2,1,0:T(8,128)(2,1)} %value_hbm.1, bf16[2048]{0:T(1024)(128)(2,1)} %norm_gain_hbm.1, ...), custom_call_target="tpu_custom_call" | custom-call | tf_op jit(solution)/shard_map/layer/pallas_call | solution.py:499
  39.8 0.6 %finish.1 = (bf16[8,2048]{1,0:T(8,128)(2,1)}, bf16[8,128]{1,0:T(8,128)(2,1)}, bf16[8,128]{1,0:T(8,128)(2,1)}) custom-call(bf16[8,2048]{1,0:T(8,128)(2,1)S(1)} %get-tuple-element.6.mixed_in, bf16[8,128]{1,0:T(8,128)(2,1)S(1)} %get-tuple-element.7.newk_in, bf16[8,128]{1,0:T(8,128)(2,1)S(1)} %get-tuple-element.8.newv_in), custom_call_target="tpu_custom_call" | custom-call | tf_op jit(solution)/shard_map/finish/pallas_call | solution.py:510
